TPU v7x, 256 devices: a whole 4x4x8 slice. The times are simulated.
256 devices in a mesh: ep: 128 (over z, y, x), tp: 2 (over core).
Axes of the slice: x: 4, y: 4, z: 8, core: 2. Of those that a mesh axis runs over, the one named last changes fastest.
Arguments:
- tokens: bfloat16 [2048, 1024], P('ep'), may hold values from -6 to 6
- lengths: int32 [2048], P('ep'), may hold values from 1 to 1024, 1048576 in all
- routes: int32 [2048, 2], replicated, may hold values from 0 to 15, all different within a row; in each aligned block of 16 rows (0 to 15, 16 to 31, ...) at most 4 rows name the same one
- route_weights: float32 [2048, 2], replicated, may hold values from 0.1 to 1
- key_cache: bfloat16 [2048, 1024, 256], P('ep', None, 'tp'), may hold values from -6 to 6
- value_cache: bfloat16 [2048, 1024, 256], P('ep', None, 'tp'), may hold values from -6 to 6
- w_query: bfloat16 [1024, 1024], P(None, 'tp'), may hold values from -0.1875 to 0.1875
- w_key: bfloat16 [1024, 256], P(None, 'tp'), may hold values from -0.1875 to 0.1875
- w_value: bfloat16 [1024, 256], P(None, 'tp'), may hold values from -0.1875 to 0.1875
- w_out: bfloat16 [1024, 1024], P('tp'), may hold values from -0.1875 to 0.1875
- score_offset: float32 [16], P('tp'), may hold values from -9 to -3
- attn_gain: float32 [1024], replicated, may hold values from 0.1 to 1.9
- ffn_gain: float32 [1024], replicated, may hold values from 0.1 to 1.9
- w_gate: bfloat16 [1024, 114688], P(None, ('ep', 'tp')), may hold values from -0.1875 to 0.1875
- w_up: bfloat16 [1024, 114688], P(None, ('ep', 'tp')), may hold values from -0.1875 to 0.1875
- w_down: bfloat16 [114688, 1024], P(('ep', 'tp')), may hold values from -0.0625 to 0.0625
Outputs:
- layer_out: bfloat16 [2048, 1024], P('ep', 'tp')
- new_keys: bfloat16 [2048, 256], P('ep', 'tp')
- new_values: bfloat16 [2048, 256], P('ep', 'tp')
Inputs may be any that keep to these rules, and one draw needn't show every extreme that they name: `routes`: each row names 2 different experts. Among the rows of one index of ep (aligned blocks of 16 rows) no expert is named by more than 4 rows, and in some block one expert is named by exactly 4 rows.
All inputs are finite; a program needn't handle non-finite values. No bound on the sum of `lengths` on one device may be relied on, other than what follows from the above.
Results may differ from a plain program's by a relative error of at most 0.0095.
Values may be sent and summed in bfloat16 or wider, within the bound.
No kernel may reach another device: no remote copies, remote signals or barrier semaphores. Data moves between devices by JAX's collectives and lax.ppermute only.
A program may use at most 128 MiB of HBM per device.

v0:
```python
import math

import jax
import jax.numpy as jnp
from jax import lax
from jax.sharding import PartitionSpec as P

HEAD_DIM = 64
EXPERTS = 16


norm_eps = 1e-06


def total_of_pieces(x, axis):
    parts = lax.all_gather(x, axis).astype(jnp.float32)
    return parts.sum(axis=0)


def cut_along(x, dim, devices):
    dims = x.shape
    parts = x.reshape(*dims[:dim], devices, dims[dim] // devices, *dims[dim + 1 :])
    return jnp.moveaxis(parts, dim, 0)


def summed_on_arrival(x, axis, dim):
    devices = lax.axis_size(axis)
    parts = lax.all_to_all(cut_along(x, dim, devices), axis, 0, 0, tiled=True)
    return jnp.sum(parts.astype(jnp.float32), axis=0)


def rms_rows(values, gain_row):
    widened = values.astype(jnp.float32)
    scaled = widened * lax.rsqrt(jnp.mean(widened * widened, axis=-1, keepdims=True) + norm_eps)
    return (scaled * gain_row).astype(jnp.bfloat16)


def expert_rows(inputs, gate_cols, up_cols, down_rows):
    gate = jnp.dot(inputs, gate_cols, preferred_element_type=jnp.float32)
    upward = jnp.dot(inputs, up_cols, preferred_element_type=jnp.float32)
    hidden = (jax.nn.silu(gate) * upward).astype(jnp.bfloat16)
    return jnp.dot(hidden, down_rows, preferred_element_type=jnp.float32)


def later_sums(log_fail):
    dims_shape = log_fail.shape
    context = dims_shape[-1]
    span_width = math.gcd(context, 128)
    block_count = context // span_width
    blocks = log_fail.reshape(dims_shape[:-1] + (block_count, span_width))
    position_ids = jnp.arange(span_width, dtype=jnp.int32)
    inside_mask = (position_ids[:, None] > position_ids[None, :]).astype(jnp.float32)
    within = jnp.einsum("...cw,wv->...cv", blocks, inside_mask)
    totals = jnp.sum(blocks, axis=-1)
    block_ids = jnp.arange(block_count, dtype=jnp.int32)
    across_mask = (block_ids[:, None] > block_ids[None, :]).astype(jnp.float32)
    carried = jnp.einsum("...c,cb->...b", totals, across_mask)
    return (within + carried[..., None]).reshape(dims_shape)


def code_slots(expert_ids, capacity):
    onehot = (expert_ids[..., None] == jnp.arange(EXPERTS, dtype=jnp.int32)).astype(jnp.int32)
    before = jnp.cumsum(onehot, axis=-2) - onehot
    slot_index = jnp.sum(before * onehot, axis=-1)
    return expert_ids * capacity + slot_index


def shards(
    tokens,
    lengths,
    routes,
    route_weights,
    key_cache,
    value_cache,
    w_query,
    w_key,
    w_value,
    w_out,
    score_offset,
    attn_gain,
    ffn_gain,
    w_gate,
    w_up,
    w_down,
):
    seq_count = tokens.shape[0]
    model_width = tokens.shape[1]
    context = key_cache.shape[1]
    kv_local = key_cache.shape[2] // HEAD_DIM
    heads_local = w_query.shape[1] // HEAD_DIM
    group_size = heads_local // kv_local
    normed = rms_rows(tokens, attn_gain)
    queries = jnp.dot(normed, w_query, preferred_element_type=jnp.float32).astype(jnp.bfloat16)
    new_keys = jnp.dot(normed, w_key, preferred_element_type=jnp.float32).astype(jnp.bfloat16)
    new_values = jnp.dot(normed, w_value, preferred_element_type=jnp.float32).astype(jnp.bfloat16)
    query_heads = queries.reshape(seq_count, kv_local, group_size, HEAD_DIM)
    cache_keys = key_cache.reshape(seq_count, context, kv_local, HEAD_DIM)
    cache_values = value_cache.reshape(seq_count, context, kv_local, HEAD_DIM)
    scores = jnp.einsum(
        "bkgd,bskd->bkgs", query_heads, cache_keys, preferred_element_type=jnp.float32
    )
    scores = (
        scores * HEAD_DIM ** (-0.5) + score_offset.reshape(kv_local, group_size)[None, :, :, None]
    )
    valid = jnp.arange(context, dtype=jnp.int32)[None, None, None, :] < lengths[:, None, None, None]
    log_fail = jnp.where(valid, jax.nn.log_sigmoid(-scores), 0.0)
    after = later_sums(log_fail)
    stick = jnp.where(valid, jnp.exp(jax.nn.log_sigmoid(scores) + after), 0.0).astype(jnp.bfloat16)
    attended = jnp.einsum(
        "bkgs,bskd->bkgd", stick, cache_values, preferred_element_type=jnp.float32
    )
    attended = attended.astype(jnp.bfloat16).reshape(seq_count, heads_local * HEAD_DIM)
    partial_part = jnp.dot(attended, w_out, preferred_element_type=jnp.float32)
    middle = (
        tokens.astype(jnp.float32)
        + total_of_pieces(partial_part.astype(jnp.bfloat16), "tp").astype(jnp.float32)
    ).astype(jnp.bfloat16)
    moe_in = rms_rows(middle, ffn_gain)
    top_count = routes.shape[1]
    capacity = max(2, 2 * seq_count * top_count // EXPERTS)
    sources = lax.axis_size("ep")
    span_size = sources // EXPERTS
    half_width = model_width // lax.axis_size("tp")
    ep_index = lax.axis_index("ep")
    tp_index = lax.axis_index("tp")
    own_routes = lax.dynamic_slice_in_dim(routes, ep_index * seq_count, seq_count, 0)
    own_weights = lax.dynamic_slice_in_dim(route_weights, ep_index * seq_count, seq_count, 0)
    own_codes = code_slots(own_routes.reshape(-1), capacity)
    slot_range = jnp.arange(EXPERTS * capacity, dtype=jnp.int32)
    picker = (slot_range[:, None] == own_codes[None, :]).astype(jnp.bfloat16)
    spread = jnp.repeat(moe_in, top_count, axis=0)
    outgoing = jnp.dot(picker, spread, preferred_element_type=jnp.float32).astype(jnp.bfloat16)
    outgoing = jnp.repeat(outgoing.reshape(EXPERTS, capacity, model_width), span_size, axis=0)
    arrived = lax.all_to_all(outgoing, "ep", split_axis=0, concat_axis=0, tiled=True)
    slot_count = arrived.shape[1]
    expert_term = expert_rows(arrived.reshape(-1, model_width), w_gate, w_up, w_down)
    expert_term = expert_term.reshape(sources, slot_count, model_width)
    shares = summed_on_arrival(expert_term.astype(jnp.bfloat16), "tp", 2)
    returned = lax.all_to_all(
        shares.astype(jnp.bfloat16), "ep", split_axis=0, concat_axis=0, tiled=True
    ).astype(shares.dtype)
    results = jnp.sum(returned.reshape(EXPERTS, span_size, capacity, half_width), axis=1)
    results = results.reshape(EXPERTS * capacity, half_width)
    matched = slot_range[None, None, :] == own_codes.reshape(seq_count, top_count)[:, :, None]
    weighted = jnp.sum(jnp.where(matched, own_weights[:, :, None], 0.0), axis=1)
    mixture = jnp.dot(weighted, results)
    own_middle = lax.dynamic_slice_in_dim(middle, tp_index * half_width, half_width, 1)
    layer_out = (own_middle.astype(jnp.float32) + mixture).astype(jnp.bfloat16)
    return (layer_out, new_keys, new_values)


def solution(mesh):
    in_specs = (
        P("ep", None),
        P("ep"),
        P(),
        P(),
        P("ep", None, "tp"),
        P("ep", None, "tp"),
        P(None, "tp"),
        P(None, "tp"),
        P(None, "tp"),
        P("tp", None),
        P("tp"),
        P(),
        P(),
        P(None, ("ep", "tp")),
        P(None, ("ep", "tp")),
        P(("ep", "tp"), None),
    )
    out_specs = (P("ep", "tp"), P("ep", "tp"), P("ep", "tp"))
    return jax.shard_map(shards, mesh=mesh, in_specs=in_specs, out_specs=out_specs, check_vma=False)
```

profile of v0, /device:TPU:1, one launch (start us, length us, event | category | flops | bytes accessed | tf_op | source)
XLA Modules:
  0.0 118.8 jit_solution(5837329286921709950)
XLA Ops:
  0.7 0.8 constant_dynamic-slice_fusion.1
  1.8 0.2 select_reduce_fusion.1
  2.0 0.9 fusion.22
  2.9 1.6 %convolution_convert_fusion.4 = bf16[16,512]{1,0:T(8,128)(2,1)S(1)} fusion(bf16[1024,512]{1,0:T(8,128)(2,1)} %param.22, bf16[16,1024]{1,0:T(8,128)(2,1)} %param.16, f32[1024]{0:T(1024)} %param.27, f32[16]{0:T(128)S(1)} %add_rsqrt_fusion.1), kind=kOutput, calls=%fused_computation.13 | convolution fusion | flops 16850944 | bytes 1101888 | tf_op jit(solution)/shard_map/dot_general | solution.py:93
  4.5 0.7 iota_compare_fusion.1
  5.3 6.4 %copy.51 = bf16[16,1024,128]{1,2,0:T(8,128)(2,1)} copy(bf16[16,1024,128]{2,1,0:T(8,128)(2,1)} %param.20) | data formatting | bytes 8388608 | tf_op args[4]
  11.8 3.2 %fusion.14 = (f32[16,2,4,1024]{3,2,1,0:T(4,128)S(1)}, f32[16,2,4,1024]{3,2,1,0:T(4,128)S(1)}) fusion(pred[16,1024]{1,0:T(8,128)(4,1)S(1)} %iota_compare_fusion.1, f32[2,4]{1,0:T(2,128)S(1)} %add.74, bf16[16,2,4,64]{3,2,1,0:T(4,128)(2,1)S(1)} %reshape.107, bf16[16,1024,2,64]{1,3,2,0:T(8,128)(2,1)} %bitcast.40), kind=kOutput, calls=%fused_computation.29 | convolution fusion | flops 18087936 | bytes 5275680 | tf_op jit(solution)/shard_map/bkgd,bskd->bkgs/dot_general | solution.py:99
  15.0 0.2 reshape.109
  15.2 0.3 reduce_sum.78
  15.5 0.2 fusion.26
  15.8 0.2 convolution_add_fusion
  16.1 0.2 reshape.110
  16.2 6.4 %copy.54 = bf16[16,1024,128]{1,2,0:T(8,128)(2,1)} copy(bf16[16,1024,128]{2,1,0:T(8,128)(2,1)} %param.21) | data formatting | bytes 8388608 | tf_op args[5]
  22.7 3.4 %convolution_convert_fusion.3 = bf16[16,2,4,64]{3,2,1,0:T(4,128)(2,1)S(1)} fusion(bf16[16,1024,2,64]{1,3,2,0:T(8,128)(2,1)} %bitcast.41, f32[16,2,4,1024]{3,2,1,0:T(4,128)S(1)} %reshape.110, f32[16,2,4,1024]{3,2,1,0:T(4,128)S(1)} %get-tuple-element.6, pred[16,1024]{1,0:T(8,128)(4,1)S(1)} %iota_compare_fusion.1), kind=kOutput, calls=%fused_computation.10 | convolution fusion | flops 18227200 | bytes 5275648 | tf_op jit(solution)/shard_map/bkgs,bskd->bkgd/dot_general | solution.py:109
  26.2 0.2 convolution_convert_fusion.2
  26.4 4.7 %all-gather = bf16[32,1024]{1,0:T(8,128)(2,1)S(1)} all-gather(bf16[16,1024]{1,0:T(8,128)(2,1)S(1)} %convolution_convert_fusion.2), channel_id=2, replica_groups=mesh['ep'=128,'tp'=2] {'tp'}, dimensions={0}, use_global_device_ids=true | all-gather | bytes 98304 | tf_op jit(solution)/shard_map/all_gather | solution.py:16
  31.7 0.3 broadcast_in_dim.52
  32.0 42.8 %all_to_all.15 = bf16[128,4,1024]{2,1,0:T(4,128)(2,1)S(1)} all-to-all(bf16[128,4,1024]{2,1,0:T(4,128)(2,1)S(1)} %bitcast.42), channel_id=1, replica_groups=mesh['ep'=128,'tp'=2] {'ep'}, dimensions={0} | all-to-all | bytes 2097152 | tf_op jit(solution)/shard_map/all_to_all | solution.py:134
  74.7 0.3 reshape.116
  75.0 1.9 %fusion.40 = f32[512,448]{0,1:T(8,128)S(1)} fusion(bf16[512,1024]{1,0:T(8,128)(2,1)S(1)} %reshape.116, bf16[1024,448]{0,1:T(8,128)(2,1)} %param.29), kind=kOutput, calls=%fused_computation.68 | convolution fusion | flops 469762048 | bytes 2883584 | tf_op jit(solution)/shard_map/dot_general | solution.py:39
  76.9 3.8 %convolution_convert_fusion = bf16[512,1024]{1,0:T(8,128)(2,1)} fusion(bf16[448,1024]{1,0:T(8,128)(2,1)} %param.31, bf16[512,1024]{1,0:T(8,128)(2,1)S(1)} %reshape.116, bf16[1024,448]{0,1:T(8,128)(2,1)} %param.30, f32[512,448]{0,1:T(8,128)S(1)} %fusion.40), kind=kOutput, calls=%fused_computation.2 | convolution fusion | flops 941424640 | bytes 4849664 | tf_op jit(solution)/shard_map/dot_general | solution.py:42
  80.7 1.9 %convert_element_type.80 = bf16[128,4,2,512]{3,2,1,0:T(2,128)(2,1)S(1)} reshape(bf16[512,1024]{1,0:T(8,128)(2,1)} %convolution_convert_fusion) | data formatting | bytes 2097152 | tf_op jit(solution)/shard_map/convert_element_type | solution.py:138
  82.6 0.4 copy.68
  83.0 7.2 %all_to_all.16 = bf16[2,128,4,512]{3,2,1,0:T(4,128)(2,1)S(1)} all-to-all(bf16[2,128,4,512]{3,2,1,0:T(4,128)(2,1)S(1)} %bitcast.43), channel_id=1, replica_groups=mesh['ep'=128,'tp'=2] {'tp'}, dimensions={0} | all-to-all | bytes 2097152 | tf_op jit(solution)/shard_map/all_to_all | solution.py:28
  90.3 1.9 %reduce_sum.84 = bf16[128,4,512]{2,1,0:T(4,128)(2,1)} reduce(bf16[2,128,4,512]{3,2,1,0:T(4,128)(2,1)S(1)} %all_to_all.16, bf16[]{:T(256)} %constant.42.clone.1), dimensions={0}, to_apply=%region_7.8 | reduce | flops 262144 | bytes 1572866 | tf_op jit(solution)/shard_map/reduce_sum | solution.py:29
  92.2 6.2 %all-to-all-start.2 = ((bf16[128,4,512]{2,1,0:T(4,128)(2,1)}), bf16[128,4,512]{2,1,0:T(4,128)(2,1)S(1)}, u32[]{:S(2)}, u32[]{:S(2)}) async-start(bf16[128,4,512]{2,1,0:T(4,128)(2,1)} %reduce_sum.84), calls=%async_computation.2 | async-start | bytes 1048576 | tf_op jit(solution)/shard_map/all_to_all | solution.py:139
  98.5 0.8 constant_dynamic-slice_fusion
  99.4 0.8 convolution_convert_fusion.5
  100.2 0.8 convolution_convert_fusion.6
  101.0 16.5 %all-to-all-done.2 = bf16[128,4,512]{2,1,0:T(4,128)(2,1)S(1)} async-done(((bf16[128,4,512]{2,1,0:T(4,128)(2,1)}), bf16[128,4,512]{2,1,0:T(4,128)(2,1)S(1)}, u32[]{:S(2)}, u32[]{:S(2)}) %all-to-all-start.2) | async-done | bytes 524320 | tf_op jit(solution)/shard_map/all_to_all | solution.py:139
  117.5 0.4 convert_reduce_fusion
  118.0 0.7 fusion.2
  (38 shorter events, 1.6 us)
Async XLA Ops:
  0.6 25.5 %copy-start = (bf16[512,1024]{1,0:T(8,128)(2,1)S(1)}, bf16[512,1024]{1,0:T(8,128)(2,1)}, u32[]{:S(2)}) copy-start(bf16[512,1024]{1,0:T(8,128)(2,1)} %param.25) | copy-start | bytes 3145732
  5.3 6.4 %copy-start.6 = (f32[8]{0:T(128)S(1)}, f32[8]{0:T(128)}, u32[]{:S(2)}) copy-start(f32[8]{0:T(128)} %param.26) | copy-start | bytes 100
  22.6 8.5 %copy-start.1 = (bf16[16,1024]{1,0:T(8,128)(2,1)S(1)}, bf16[16,1024]{1,0:T(8,128)(2,1)}, u32[]{:S(2)}) copy-start(bf16[16,1024]{1,0:T(8,128)(2,1)} %param.16) | copy-start | bytes 98308
  22.6 8.6 %copy-start.3 = (f32[1024]{0:T(1024)S(1)}, f32[1024]{0:T(1024)}, u32[]{:S(2)}) copy-start(f32[1024]{0:T(1024)} %param.28) | copy-start | bytes 12292
  80.7 18.7 %copy-start.2 = (f32[1024]{0:T(1024)S(1)}, f32[1024]{0:T(1024)}, u32[]{:S(2)}) copy-start(f32[1024]{0:T(1024)} %param.27) | copy-start | bytes 12292
  80.7 18.7 %copy-start.4 = (bf16[1024,128]{1,0:T(8,128)(2,1)S(1)}, bf16[1024,128]{1,0:T(8,128)(2,1)}, u32[]{:S(2)}) copy-start(bf16[1024,128]{1,0:T(8,128)(2,1)} %param.24) | copy-start | bytes 786436
  80.7 19.5 %copy-start.5 = (bf16[1024,128]{1,0:T(8,128)(2,1)S(1)}, bf16[1024,128]{1,0:T(8,128)(2,1)}, u32[]{:S(2)}) copy-start(bf16[1024,128]{1,0:T(8,128)(2,1)} %param.23) | copy-start | bytes 786436
  92.2 25.4 %all-to-all-start.2 = ((bf16[128,4,512]{2,1,0:T(4,128)(2,1)}), bf16[128,4,512]{2,1,0:T(4,128)(2,1)S(1)}, u32[]{:S(2)}, u32[]{:S(2)}) async-start(bf16[128,4,512]{2,1,0:T(4,128)(2,1)} %reduce_sum.84), calls=%async_computation.2 | async-start | bytes 1048576 | tf_op jit(solution)/shard_map/all_to_all | solution.py:139
where the time goes:
time: 119 us
  blocking collectives  54.7 us (46%)
  local copies, waits for them, and re-layouts  18.7 us (16%)
  matrix products  17 us (14%)
  waiting for transfers between devices  16.5 us (14%)
  starting transfers between devices  6.17 us (5%)
  other arithmetic  4.81 us (4%)
    all_to_all x1, blocking collectives, shards(): lax.all_to_all(outgoing, 'ep', split_axis=0, concat_axis=0, tiled=True)  42.8 us
    all_to_all x1, waiting for transfers between devices, shards(): lax.all_to_all(shares.astype(jnp.bfloat16), 'ep', split_axis=0, concat_ax...  16.5 us
    unnamed x18, local copies, waits for them, and re-layouts  13 us
    all_to_all x1, blocking collectives, summed_on_arrival(): parts = lax.all_to_all(cut_along(x, dim, devices), axis, 0, 0, tiled=True)  7.25 us
    all_to_all x1, starting transfers between devices, shards(): lax.all_to_all(shares.astype(jnp.bfloat16), 'ep', split_axis=0, concat_ax...  6.17 us
    all_gather x1, blocking collectives, total_of_pieces(): parts = lax.all_gather(x, axis).astype(jnp.float32)  4.7 us
    dot_general x1, matrix products, expert_rows(): return jnp.dot(hidden, down_rows, preferred_element_type=jnp.float32)  3.82 us
    dot_general x1, matrix products, shards(): jnp.einsum('bkgs,bskd->bkgd', stick, cache_values, preferred_element_type...  3.4 us
  transfers between devices with their start and end apart: 1, of which 1 were waited for; matrix products, arithmetic and copies ran while one was open for 2% of the time, Pallas kernels for 0%

commit v1 on v0

v1 whole, which is shorter than its diff:
```python
import jax
import jax.numpy as jnp
from jax import lax
from jax.experimental import pallas as pl
from jax.experimental.pallas import tpu as pltpu
from jax.sharding import PartitionSpec as P

HEAD_DIM = 64
EXPERTS = 16
LANES = 128
norm_eps = 1e-06

f32 = jnp.float32
bf16 = jnp.bfloat16


def rms_rows(values, gain_row):
    widened = values.astype(f32)
    scaled = widened * lax.rsqrt(jnp.mean(widened * widened, axis=-1, keepdims=True) + norm_eps)
    return (scaled * gain_row).astype(bf16)


def dot(a, b, dims=((1,), (0,))):
    return lax.dot_general(a, b, (dims, ((), ())), preferred_element_type=f32)


def split_two(x):
    high = x.astype(bf16)
    return high, (x - high.astype(f32)).astype(bf16)


def iota(shape, dim):
    return lax.broadcasted_iota(jnp.int32, shape, dim)


def attention_kernel(
    lengths_hbm,
    offsets_hbm,
    tokens_hbm,
    gain_hbm,
    key_hbm,
    value_hbm,
    wq_hbm,
    wk_hbm,
    wv_hbm,
    wo_hbm,
    part_out,
    keys_out,
    values_out,
    lengths,
    offsets,
    tokens,
    gain,
    kbuf,
    vbuf,
    wq,
    wk,
    wv,
    wo,
    qrows,
    arows,
    wsem,
    ksem,
    vsem,
):
    seqs, context, width = kbuf.shape
    heads = qrows.shape[0] // seqs
    pairs = seqs // 2
    blocks = context // LANES

    def key_copy(p):
        return pltpu.make_async_copy(key_hbm.at[pl.ds(2 * p, 2)], kbuf.at[pl.ds(2 * p, 2)], ksem.at[p])

    def value_copy(p):
        return pltpu.make_async_copy(value_hbm.at[pl.ds(2 * p, 2)], vbuf.at[pl.ds(2 * p, 2)], vsem.at[p])

    first_copies = (
        (wq_hbm, wq),
        (wk_hbm, wk),
        (wv_hbm, wv),
        (wo_hbm, wo),
        (tokens_hbm, tokens),
        (gain_hbm, gain),
        (lengths_hbm, lengths),
        (offsets_hbm, offsets),
    )
    weights = [pltpu.make_async_copy(src, dst, wsem.at[i]) for i, (src, dst) in enumerate(first_copies)]
    for copy in weights[4:] + weights[:3]:
        copy.start()
    for p in range(pairs):
        key_copy(p).start()
        value_copy(p).start()
    weights[3].start()

    for copy in weights[4:]:
        copy.wait()
    normed = rms_rows(tokens[...], gain[...])
    weights[0].wait()
    queries = dot(normed, wq[...]).astype(bf16).astype(f32)
    lane = iota((seqs, LANES), 1)
    for h in range(heads):
        tile = queries[:, (h // 2) * LANES : (h // 2 + 1) * LANES]
        upper = h >= heads // 2
        if (h % 2 == 1) != upper:
            tile = pltpu.roll(tile, HEAD_DIM, 1)
        tile = jnp.where((lane >= HEAD_DIM) == upper, tile, 0.0)
        qrows[pl.ds(h, seqs, stride=heads), :] = tile
    weights[1].wait()
    keys_out[...] = dot(normed, wk[...]).astype(bf16)
    weights[2].wait()
    values_out[...] = dot(normed, wv[...]).astype(bf16)

    rows = 2 * heads
    head_of = iota((rows, LANES), 0) % heads
    offset = jnp.zeros((rows, LANES), f32)
    for h in range(heads):
        offset = jnp.where(head_of == h, offsets[h], offset)
    first = iota((rows, LANES), 0) < heads
    tri_row = iota((2 * LANES, 2 * LANES), 0) % LANES
    tri_col = iota((2 * LANES, 2 * LANES), 1)
    later = jnp.where((tri_row > tri_col) | (tri_col >= LANES), 1.0, 0.0).astype(bf16)
    position = iota((rows, LANES), 1)
    zero = jnp.zeros((heads, LANES), f32)

    def one_pair(p, carry):
        key_copy(p).wait()
        base = pl.multiple_of(p * rows, rows)
        both = qrows[pl.ds(base, rows), :]
        left = jnp.concatenate([both[:heads], zero], axis=0)
        right = jnp.concatenate([zero, both[heads:]], axis=0)
        query = jnp.concatenate([left, right], axis=1).astype(bf16)
        keys = jnp.concatenate([kbuf[2 * p], kbuf[2 * p + 1]], axis=1)
        scores = dot(query, keys, ((1,), (1,)))
        limit = jnp.where(first, lengths[2 * p], lengths[2 * p + 1])
        taken = []
        highs = []
        lows = []
        for c in range(blocks):
            z = scores[:, c * LANES : (c + 1) * LANES] * HEAD_DIM ** (-0.5) + offset
            tail = jnp.log1p(jnp.exp(-jnp.abs(z)))
            fail = jnp.where(position + c * LANES < limit, -(jnp.maximum(z, 0.0) + tail), 0.0)
            taken.append(jnp.minimum(z, 0.0) - tail)
            high, low = split_two(fail)
            highs.append(high)
            lows.append(low)
        halves = jnp.concatenate([jnp.concatenate(highs, axis=0), jnp.concatenate(lows, axis=0)], axis=1)
        sums = dot(halves, later)
        carried = jnp.zeros((rows, LANES), f32)
        sticks = [None] * blocks
        for c in reversed(range(blocks)):
            block = sums[c * rows : (c + 1) * rows]
            share = jnp.exp(taken[c] + (block[:, :LANES] + carried))
            sticks[c] = jnp.where(position + c * LANES < limit, share, 0.0).astype(bf16)
            carried = carried + block[:, LANES:]
        stick = jnp.concatenate(sticks, axis=1)
        value_copy(p).wait()
        values = jnp.concatenate([vbuf[2 * p], vbuf[2 * p + 1]], axis=1)
        attended = dot(stick, values)
        arows[pl.ds(base, rows), :] = jnp.where(first, attended[:, :LANES], attended[:, LANES:])
        return carry

    lax.fori_loop(0, pairs, one_pair, 0)

    tiles = []
    for q in range(heads // 2):
        upper = 2 * q >= heads // 2
        even = arows[pl.ds(2 * q, seqs, stride=heads), :]
        odd = arows[pl.ds(2 * q + 1, seqs, stride=heads), :]
        if upper:
            even = pltpu.roll(even, HEAD_DIM, 1)
        else:
            odd = pltpu.roll(odd, HEAD_DIM, 1)
        tiles.append(jnp.where(lane < HEAD_DIM, even, odd))
    attended = jnp.concatenate(tiles, axis=1).astype(bf16)
    weights[3].wait()
    part_out[...] = dot(attended, wo[...]).astype(bf16)


def attention(lengths, offsets, tokens, gain, key_cache, value_cache, w_query, w_key, w_value, w_out):
    seqs, width = tokens.shape
    heads = offsets.shape[0]
    kv = w_key.shape[1]
    vmem = pl.BlockSpec(memory_space=pltpu.VMEM)
    hbm = pl.BlockSpec(memory_space=pltpu.HBM)
    caches = [
        pltpu.with_memory_space_constraint(x, pltpu.HBM)
        for x in (lengths, offsets, tokens, gain, key_cache, value_cache, w_query, w_key, w_value, w_out)
    ]
    return pl.pallas_call(
        attention_kernel,
        out_shape=(
            jax.ShapeDtypeStruct((seqs, width), bf16),
            jax.ShapeDtypeStruct((seqs, kv), bf16),
            jax.ShapeDtypeStruct((seqs, kv), bf16),
        ),
        in_specs=[hbm] * 10,
        out_specs=(vmem, vmem, vmem),
        scratch_shapes=[
            pltpu.SMEM(lengths.shape, jnp.int32),
            pltpu.SMEM(offsets.shape, f32),
            pltpu.VMEM(tokens.shape, bf16),
            pltpu.VMEM(gain.shape, f32),
            pltpu.VMEM(key_cache.shape, bf16),
            pltpu.VMEM(value_cache.shape, bf16),
            pltpu.VMEM(w_query.shape, bf16),
            pltpu.VMEM(w_key.shape, bf16),
            pltpu.VMEM(w_value.shape, bf16),
            pltpu.VMEM(w_out.shape, bf16),
            pltpu.VMEM((seqs * heads, LANES), f32),
            pltpu.VMEM((seqs * heads, LANES), f32),
            pltpu.SemaphoreType.DMA((8,)),
            pltpu.SemaphoreType.DMA((seqs // 2,)),
            pltpu.SemaphoreType.DMA((seqs // 2,)),
        ],
        compiler_params=pltpu.CompilerParams(vmem_limit_bytes=32 << 20),
        name="attention",
    )(*caches)


def dispatch_kernel(
    tokens, gain, own, peer, routes_hbm, weights_hbm, rows_out, middle_out, mix_out, route, weight, sems
):
    seqs, width = tokens.shape
    slots, half = rows_out.shape
    capacity = slots // EXPERTS
    start = lax.axis_index("ep") * seqs
    tile = pl.multiple_of(start // LANES * LANES, LANES)
    copies = [
        pltpu.make_async_copy(routes_hbm.at[:, pl.ds(tile, LANES)], route, sems.at[0]),
        pltpu.make_async_copy(weights_hbm.at[:, pl.ds(tile, LANES)], weight, sems.at[1]),
    ]
    for copy in copies:
        copy.start()
    low_half = lax.axis_index("tp") == 0
    middle = (tokens[...].astype(f32) + own[...].astype(f32) + peer[...].astype(f32)).astype(bf16)
    moe_in = rms_rows(middle, gain[...]).astype(f32)
    mine = jnp.where(low_half, moe_in[:, :half], moe_in[:, half:]).astype(bf16)
    middle = middle.astype(f32)
    middle_out[...] = jnp.where(low_half, middle[:, :half], middle[:, half:]).astype(bf16)
    for copy in copies:
        copy.wait()
    here = iota((seqs, LANES), 1) == iota((seqs, LANES), 0) + (start - tile)

    def column(values):
        return jnp.sum(jnp.where(here, values, 0.0), axis=1, keepdims=True)

    r0, r1 = (column(route[i : i + 1, :].astype(f32)) for i in range(2))
    w0, w1 = (column(weight[i : i + 1, :]) for i in range(2))
    earlier = jnp.where(iota((seqs, seqs), 1) < iota((seqs, seqs), 0), 1.0, 0.0).astype(bf16)

    def slot_mask(expert, slot):
        expert = expert.astype(f32)
        first = r0 == expert
        named = first | (r1 == expert)
        before = dot(earlier, jnp.where(named, 1.0, 0.0).astype(bf16))
        return first, named & (before == slot.astype(f32))

    index = iota((seqs, slots), 1)
    _, chosen = slot_mask(index // capacity, index % capacity)
    rows_out[...] = dot(jnp.where(chosen, 1.0, 0.0).astype(bf16), mine, ((0,), (0,))).astype(bf16)
    returned = mix_out.shape[1]
    index = iota((seqs, returned), 1)
    first, chosen = slot_mask(index // (returned // EXPERTS), index % capacity)
    high, low = split_two(jnp.where(chosen, jnp.where(first, w0, w1), 0.0))
    mix_out[...] = jnp.concatenate([high, low], axis=0)


def dispatch(tokens, gain, own, peer, routes, weights, capacity, sources):
    seqs, width = tokens.shape
    vmem = pl.BlockSpec(memory_space=pltpu.VMEM)
    hbm = pl.BlockSpec(memory_space=pltpu.HBM)
    outs = ((EXPERTS * capacity, width // 2), (seqs, width // 2), (2 * seqs, sources * capacity))
    return pl.pallas_call(
        dispatch_kernel,
        out_shape=tuple(jax.ShapeDtypeStruct(shape, bf16) for shape in outs),
        in_specs=[vmem] * 4 + [hbm] * 2,
        out_specs=(vmem,) * 3,
        scratch_shapes=[
            pltpu.VMEM((2, LANES), jnp.int32),
            pltpu.VMEM((2, LANES), f32),
            pltpu.SemaphoreType.DMA((2,)),
        ],
        compiler_params=pltpu.CompilerParams(vmem_limit_bytes=8 << 20),
        name="dispatch",
    )(tokens, gain, own, peer, routes, weights)


def expert_kernel(own, peer, gate_w, up_w, down_w, keep_out, send_out):
    half = own.shape[1]
    tp_index = lax.axis_index("tp")
    mine = pl.multiple_of(tp_index * half, half)
    other = pl.multiple_of((1 - tp_index) * half, half)
    x, y = own[...], peer[...]

    def project(w):
        return dot(x, w[:, pl.ds(mine, half)], ((1,), (1,))) + dot(y, w[:, pl.ds(other, half)], ((1,), (1,)))

    gate = project(gate_w)
    upward = project(up_w)
    hidden = (gate / (1.0 + jnp.exp(-gate)) * upward).astype(bf16)
    send_out[...] = dot(hidden, down_w[:, pl.ds(other, half)]).astype(bf16)
    keep_out[...] = dot(hidden, down_w[:, pl.ds(mine, half)])


def expert(own, peer, gate_w, up_w, down_w):
    vmem = pl.BlockSpec(memory_space=pltpu.VMEM)
    return pl.pallas_call(
        expert_kernel,
        out_shape=(jax.ShapeDtypeStruct(own.shape, f32), jax.ShapeDtypeStruct(own.shape, bf16)),
        in_specs=[vmem] * 5,
        out_specs=(vmem, vmem),
        compiler_params=pltpu.CompilerParams(vmem_limit_bytes=32 << 20),
        name="expert",
    )(own, peer, gate_w, up_w, down_w)


def mix_kernel(mix, returned, middle, out):
    seqs = middle.shape[0]
    both = dot(mix[...], returned[...])
    out[...] = (middle[...].astype(f32) + (both[:seqs] + both[seqs:])).astype(bf16)


def mix_rows(mix, returned, middle):
    vmem = pl.BlockSpec(memory_space=pltpu.VMEM)
    return pl.pallas_call(
        mix_kernel,
        out_shape=jax.ShapeDtypeStruct(middle.shape, bf16),
        in_specs=[vmem] * 3,
        out_specs=vmem,
        compiler_params=pltpu.CompilerParams(vmem_limit_bytes=8 << 20),
        name="mix",
    )(mix, returned, middle)


def shards(
    tokens,
    lengths,
    routes,
    route_weights,
    key_cache,
    value_cache,
    w_query,
    w_key,
    w_value,
    w_out,
    score_offset,
    attn_gain,
    ffn_gain,
    w_gate,
    w_up,
    w_down,
):
    seqs, width = tokens.shape
    sources = lax.axis_size("ep")
    span = sources // EXPERTS
    capacity = 4
    half = width // 2
    swap = [(0, 1), (1, 0)]
    part, new_keys, new_values = attention(
        lengths,
        score_offset,
        tokens,
        attn_gain.reshape(1, width),
        key_cache,
        value_cache,
        w_query,
        w_key,
        w_value,
        w_out,
    )
    other_part = lax.ppermute(part, "tp", swap)
    rows, middle, mix = dispatch(
        tokens,
        ffn_gain.reshape(1, width),
        part,
        other_part,
        routes.T,
        route_weights.T,
        capacity,
        sources,
    )
    outgoing = jnp.broadcast_to(
        rows.reshape(EXPERTS, 1, capacity, half), (EXPERTS, span, capacity, half)
    ).reshape(sources, capacity, half)
    arrived = lax.all_to_all(outgoing, "ep", split_axis=0, concat_axis=0, tiled=True)
    own = arrived.reshape(sources * capacity, half)
    peer = lax.ppermute(own, "tp", swap)
    keep, send = expert(own, peer, w_gate.T, w_up.T, w_down)
    got = lax.ppermute(send, "tp", swap)
    shares = (keep + got.astype(f32)).astype(bf16).reshape(sources, capacity, half)
    returned = lax.all_to_all(shares, "ep", split_axis=0, concat_axis=0, tiled=True)
    layer_out = mix_rows(mix, returned.reshape(sources * capacity, half), middle)
    return (layer_out, new_keys, new_values)


def solution(mesh):
    in_specs = (
        P("ep", None),
        P("ep"),
        P(),
        P(),
        P("ep", None, "tp"),
        P("ep", None, "tp"),
        P(None, "tp"),
        P(None, "tp"),
        P(None, "tp"),
        P("tp", None),
        P("tp"),
        P(),
        P(),
        P(None, ("ep", "tp")),
        P(None, ("ep", "tp")),
        P(("ep", "tp"), None),
    )
    out_specs = (P("ep", "tp"), P("ep", "tp"), P("ep", "tp"))
    return jax.shard_map(shards, mesh=mesh, in_specs=in_specs, out_specs=out_specs, check_vma=False)
```

time: 119 us -> 83.4 us (0.70)
  local copies, waits for them, and re-layouts: 18.7 us -> 1.6 us
  matrix products: 17 us -> 0 us
  Pallas kernels: 0 us -> 12.9 us
  waiting for transfers between devices: 16.5 us -> 3.93 us
  other arithmetic: 4.81 us -> 0.16 us
  blocking collectives: 54.7 us -> 57.2 us
    all_to_all x1, blocking collectives: 7.25 us -> 24.7 us  [shards(): lax.all_to_all(shares, 'ep', split_axis=0, concat_axis=0, tiled=True)]
    dot_general x12 -> x0, matrix products: 17 us -> none  [the longest x1 3.82 us: expert_rows(): return jnp.dot(hidden, down_rows, preferred_element_type=jnp.float32)]
    all_to_all x1 -> x0, waiting for transfers between devices: 16.5 us -> none  [shards(): lax.all_to_all(shares.astype(jnp.bfloat16), 'ep', split_axis=0, concat_ax...]
    unnamed x18 -> x14, local copies, waits for them, and re-layouts: 13 us -> 0.03 us
    pallas_call x0 -> x4, Pallas kernels: none -> 12.9 us  [the longest x1 9.61 us: attention(): pl.pallas_call(attention_kernel, out_shape=(jax.ShapeDtypeStruct((seqs, w...]
    all_to_all x1, blocking collectives: 42.8 us -> 32.5 us  [shards(): lax.all_to_all(outgoing, 'ep', split_axis=0, concat_axis=0, tiled=True)]
    ppermute x0 -> x3, starting transfers between devices: none -> 6.64 us  [the longest x1 3.29 us: shards(): other_part = lax.ppermute(part, 'tp', swap)]
    all_to_all x1 -> x0, starting transfers between devices: 6.17 us -> none  [shards(): lax.all_to_all(shares.astype(jnp.bfloat16), 'ep', split_axis=0, concat_ax...]
  transfers between devices with their start and end apart: 1 -> 3, of which waited for: 1 -> 3; matrix products, arithmetic and copies ran while one was open for 2% -> 0% of each run, Pallas kernels for 0% -> 0%
where the time goes in v1:
time: 83.4 us; the launch traced here: 83.2 us
  blocking collectives  57.2 us (69%)
  Pallas kernels  12.9 us (15%)
  starting transfers between devices  6.64 us (8%)
  waiting for transfers between devices  3.93 us (5%)
  local copies, waits for them, and re-layouts  1.6 us (2%)
    all_to_all x1, blocking collectives, shards(): lax.all_to_all(outgoing, 'ep', split_axis=0, concat_axis=0, tiled=True)  32.5 us
    all_to_all x1, blocking collectives, shards(): lax.all_to_all(shares, 'ep', split_axis=0, concat_axis=0, tiled=True)  24.7 us
    pallas_call x1, Pallas kernels, attention(): pl.pallas_call(attention_kernel, out_shape=(jax.ShapeDtypeStruct((seqs, w...  9.61 us
    ppermute x1, starting transfers between devices, shards(): other_part = lax.ppermute(part, 'tp', swap)  3.29 us
    ppermute x1, starting transfers between devices, shards(): peer = lax.ppermute(own, 'tp', swap)  2.87 us
    pallas_call x1, Pallas kernels, expert(): pl.pallas_call(expert_kernel, out_shape=(jax.ShapeDtypeStruct(own.shape,...  1.88 us
  transfers between devices with their start and end apart: 3, of which 3 were waited for; matrix products, arithmetic and copies ran while one was open for 0% of the time, Pallas kernels for 0%

profile of v1, /device:TPU:1, one launch (start us, length us, event | category | flops | bytes accessed | tf_op | source)
XLA Modules:
  0.0 83.2 jit_solution(203730091759236836)
XLA Ops:
  0.6 0.0 copy-start.3
  0.6 0.0 copy-start.4
  0.7 0.0 copy-start.5
  0.7 0.0 copy-start.6
  0.7 0.0 copy-start
  0.7 0.0 copy-start.1
  0.7 0.0 copy-start.2
  0.7 9.6 %attention.1 = (bf16[16,1024]{1,0:T(8,128)(2,1)S(1)}, bf16[16,128]{1,0:T(8,128)(2,1)}, bf16[16,128]{1,0:T(8,128)(2,1)}) custom-call(s32[16]{0:T(128)} %lengths_hbm.1, f32[8]{0:T(128)} %offsets_hbm.1, bf16[16,1024]{1,0:T(8,128)(2,1)} %tokens.1, f32[1,1024]{1,0:T(1,128)} %bitcast.13, bf16[16,1024,128]{2,1,0:T(8,128)(2,1)} %key_hbm.1, ...), custom_call_target="tpu_custom_call" | custom-call | tf_op jit(solution)/shard_map/attention/pallas_call | solution.py:189
  10.3 3.3 %collective-permute-start = (bf16[16,1024]{1,0:T(8,128)(2,1)S(1)}, bf16[16,1024]{1,0:T(8,128)(2,1)S(1)}, u32[]{:S(2)}, u32[]{:S(2)}) collective-permute-start(bf16[16,1024]{1,0:T(8,128)(2,1)S(1)} %get-tuple-element.11.own), channel_id=1, source_target_pairs={{0,1},{1,0},{2,3},{3,2},{4,5},{5,4},{6,7},{7,6},{8,9},{9,8},{10,11... | collective-permute-start | bytes 98312 | tf_op jit(solution)/shard_map/ppermute | solution.py:371
  13.6 0.9 %collective-permute-done.peer = bf16[16,1024]{1,0:T(8,128)(2,1)S(1)} collective-permute-done((bf16[16,1024]{1,0:T(8,128)(2,1)S(1)}, bf16[16,1024]{1,0:T(8,128)(2,1)S(1)}, u32[]{:S(2)}, u32[]{:S(2)}) %collective-permute-start) | collective-permute-done | bytes 32800 | tf_op jit(solution)/shard_map/ppermute | solution.py:371
  14.5 0.0 copy-done.3
  14.5 0.0 copy-done.4
  14.5 0.0 copy-done.5
  14.5 0.0 copy-done.6
  14.5 0.6 dispatch.1
  15.1 0.1 broadcast_in_dim.8
  15.2 32.5 %all_to_all.10 = bf16[128,4,512]{2,1,0:T(4,128)(2,1)} all-to-all(bf16[128,4,512]{2,1,0:T(4,128)(2,1)S(1)} %bitcast.12), channel_id=1, replica_groups=mesh['ep'=128,'tp'=2] {'ep'}, dimensions={0} | all-to-all | bytes 1048576 | tf_op jit(solution)/shard_map/all_to_all | solution.py:385
  47.8 1.2 %reshape.29.own = bf16[512,512]{1,0:T(8,128)(2,1)S(1)} reshape(bf16[128,4,512]{2,1,0:T(4,128)(2,1)} %all_to_all.10) | data formatting | bytes 1048576 | tf_op jit(solution)/shard_map/reshape | solution.py:386
  48.9 2.9 %collective-permute-start.1 = (bf16[512,512]{1,0:T(8,128)(2,1)S(1)}, bf16[512,512]{1,0:T(8,128)(2,1)S(1)}, u32[]{:S(2)}, u32[]{:S(2)}) collective-permute-start(bf16[512,512]{1,0:T(8,128)(2,1)S(1)} %reshape.29.own), channel_id=1, source_target_pairs={{0,1},{1,0},{2,3},{3,2},{4,5},{5,4},{6,7},{7,6},{8,9},{9,8},{10,11... | collective-permute-start | bytes 1572872 | tf_op jit(solution)/shard_map/ppermute | solution.py:387
  51.8 1.5 %collective-permute-done.1.peer = bf16[512,512]{1,0:T(8,128)(2,1)S(1)} collective-permute-done((bf16[512,512]{1,0:T(8,128)(2,1)S(1)}, bf16[512,512]{1,0:T(8,128)(2,1)S(1)}, u32[]{:S(2)}, u32[]{:S(2)}) %collective-permute-start.1) | collective-permute-done | bytes 524320 | tf_op jit(solution)/shard_map/ppermute | solution.py:387
  53.3 0.0 copy-done
  53.3 0.0 copy-done.1
  53.4 0.0 copy-done.2
  53.4 1.9 %expert.1 = (f32[512,512]{1,0:T(8,128)S(1)}, bf16[512,512]{1,0:T(8,128)(2,1)S(1)}) custom-call(bf16[512,512]{1,0:T(8,128)(2,1)S(1)} %reshape.29.own, bf16[512,512]{1,0:T(8,128)(2,1)S(1)} %collective-permute-done.1.peer, bf16[448,1024]{1,0:T(8,128)(2,1)S(1)} %bitcast.7, bf16[448,1024]{1,0:T(8,128)(2,1)S(1)} %bitcast.8, bf16[448,1024]{1,0:T(8,128)(2,1)S(1)} %copy-done.2), custom_call_target="tpu_custom_call" | custom-call | tf_op jit(solution)/shard_map/expert/pallas_call | solution.py:307
  55.2 0.5 collective-permute-start.2
  55.7 1.5 %collective-permute-done.2 = bf16[512,512]{1,0:T(8,128)(2,1)S(1)} collective-permute-done((bf16[512,512]{1,0:T(8,128)(2,1)S(1)}, bf16[512,512]{1,0:T(8,128)(2,1)S(1)}, u32[]{:S(2)}, u32[]{:S(2)}) %collective-permute-start.2) | collective-permute-done | bytes 524320 | tf_op jit(solution)/shard_map/ppermute | solution.py:389
  57.3 0.2 add_convert_fusion
  57.4 0.1 reshape.30
  57.6 24.7 %all_to_all.11 = bf16[128,4,512]{2,1,0:T(4,128)(2,1)S(1)} all-to-all(bf16[128,4,512]{2,1,0:T(4,128)(2,1)S(1)} %reshape.30), channel_id=1, replica_groups=mesh['ep'=128,'tp'=2] {'ep'}, dimensions={0} | all-to-all | bytes 1048576 | tf_op jit(solution)/shard_map/all_to_all | solution.py:391
  82.3 0.1 reshape.31.returned
  82.4 0.8 mix.1
  (1 shorter events, 0.0 us)
Async XLA Ops:
  0.6 13.8 %copy-start.3 = (bf16[16,1024]{1,0:T(8,128)(2,1)S(1)}, bf16[16,1024]{1,0:T(8,128)(2,1)}, u32[]{:S(2)}) copy-start(bf16[16,1024]{1,0:T(8,128)(2,1)} %tokens.1) | copy-start | bytes 98308
  0.6 13.8 %copy-start.4 = (s32[2048,2]{0,1:T(2,128)S(1)}, s32[2048,2]{0,1:T(2,128)}, u32[]{:S(2)}) copy-start(s32[2048,2]{0,1:T(2,128)} %param.18) | copy-start | bytes 49156
  0.7 13.8 %copy-start.5 = (f32[2048,2]{0,1:T(2,128)S(1)}, f32[2048,2]{0,1:T(2,128)}, u32[]{:S(2)}) copy-start(f32[2048,2]{0,1:T(2,128)} %param.19) | copy-start | bytes 49156
  0.7 13.8 %copy-start.6 = (f32[1024]{0:T(1024)S(1)}, f32[1024]{0:T(1024)}, u32[]{:S(2)}) copy-start(f32[1024]{0:T(1024)} %param.28) | copy-start | bytes 12292
  0.7 52.7 %copy-start = (bf16[1024,448]{0,1:T(8,128)(2,1)S(1)}, bf16[1024,448]{0,1:T(8,128)(2,1)}, u32[]{:S(2)}) copy-start(bf16[1024,448]{0,1:T(8,128)(2,1)} %param.29) | copy-start | bytes 2752516
  0.7 52.7 %copy-start.1 = (bf16[1024,448]{0,1:T(8,128)(2,1)S(1)}, bf16[1024,448]{0,1:T(8,128)(2,1)}, u32[]{:S(2)}) copy-start(bf16[1024,448]{0,1:T(8,128)(2,1)} %param.30) | copy-start | bytes 2752516
  0.7 52.7 %copy-start.2 = (bf16[448,1024]{1,0:T(8,128)(2,1)S(1)}, bf16[448,1024]{1,0:T(8,128)(2,1)}, u32[]{:S(2)}) copy-start(bf16[448,1024]{1,0:T(8,128)(2,1)} %down_w.1) | copy-start | bytes 2752516
  10.3 4.1 %collective-permute-start = (bf16[16,1024]{1,0:T(8,128)(2,1)S(1)}, bf16[16,1024]{1,0:T(8,128)(2,1)S(1)}, u32[]{:S(2)}, u32[]{:S(2)}) collective-permute-start(bf16[16,1024]{1,0:T(8,128)(2,1)S(1)} %get-tuple-element.11.own), channel_id=1, source_target_pairs={{0,1},{1,0},{2,3},{3,2},{4,5},{5,4},{6,7},{7,6},{8,9},{9,8},{10,11... | collective-permute-start | bytes 98312 | tf_op jit(solution)/shard_map/ppermute | solution.py:371
  48.9 4.4 %collective-permute-start.1 = (bf16[512,512]{1,0:T(8,128)(2,1)S(1)}, bf16[512,512]{1,0:T(8,128)(2,1)S(1)}, u32[]{:S(2)}, u32[]{:S(2)}) collective-permute-start(bf16[512,512]{1,0:T(8,128)(2,1)S(1)} %reshape.29.own), channel_id=1, source_target_pairs={{0,1},{1,0},{2,3},{3,2},{4,5},{5,4},{6,7},{7,6},{8,9},{9,8},{10,11... | collective-permute-start | bytes 1572872 | tf_op jit(solution)/shard_map/ppermute | solution.py:387
  55.2 2.0 %collective-permute-start.2 = (bf16[512,512]{1,0:T(8,128)(2,1)S(1)}, bf16[512,512]{1,0:T(8,128)(2,1)S(1)}, u32[]{:S(2)}, u32[]{:S(2)}) collective-permute-start(bf16[512,512]{1,0:T(8,128)(2,1)S(1)} %get-tuple-element.15), channel_id=1, source_target_pairs={{0,1},{1,0},{2,3},{3,2},{4,5},{5,4},{6,7},{7,6},{8,9},{9,8},{10,11... | collective-permute-start | bytes 1572872 | tf_op jit(solution)/shard_map/ppermute | solution.py:389

commit v2 on v1

--- a/solution.py
+++ b/solution.py
@@ -8,6 +8,8 @@
 HEAD_DIM = 64
 EXPERTS = 16
 LANES = 128
+GROUPS = (4, 4)
+PLANES = 8
 norm_eps = 1e-06
 
 f32 = jnp.float32
@@ -45,8 +47,8 @@
     wv_hbm,
     wo_hbm,
     part_out,
-    keys_out,
-    values_out,
+    keys_hbm,
+    values_hbm,
     lengths,
     offsets,
     tokens,
@@ -59,9 +61,13 @@
     wo,
     qrows,
     arows,
+    later,
+    new_keys,
+    new_values,
     wsem,
     ksem,
     vsem,
+    osem,
 ):
     seqs, context, width = kbuf.shape
     heads = qrows.shape[0] // seqs
@@ -87,16 +93,23 @@
     weights = [pltpu.make_async_copy(src, dst, wsem.at[i]) for i, (src, dst) in enumerate(first_copies)]
     for copy in weights[4:] + weights[:3]:
         copy.start()
-    for p in range(pairs):
-        key_copy(p).start()
-        value_copy(p).start()
-    weights[3].start()
-
     for copy in weights[4:]:
         copy.wait()
+    groups = [range(sum(GROUPS[:i]), sum(GROUPS[: i + 1])) for i in range(len(GROUPS))]
+    for members in groups:
+        if members is groups[-1]:
+            weights[3].start()
+        for p in members:
+            key_copy(p).start()
+        for p in members:
+            value_copy(p).start()
+
     normed = rms_rows(tokens[...], gain[...])
-    weights[0].wait()
+    for copy in weights[:3]:
+        copy.wait()
     queries = dot(normed, wq[...]).astype(bf16).astype(f32)
+    new_keys[...] = dot(normed, wk[...]).astype(bf16)
+    new_values[...] = dot(normed, wv[...]).astype(bf16)
     lane = iota((seqs, LANES), 1)
     for h in range(heads):
         tile = queries[:, (h // 2) * LANES : (h // 2 + 1) * LANES]
@@ -105,10 +118,12 @@
             tile = pltpu.roll(tile, HEAD_DIM, 1)
         tile = jnp.where((lane >= HEAD_DIM) == upper, tile, 0.0)
         qrows[pl.ds(h, seqs, stride=heads), :] = tile
-    weights[1].wait()
-    keys_out[...] = dot(normed, wk[...]).astype(bf16)
-    weights[2].wait()
-    values_out[...] = dot(normed, wv[...]).astype(bf16)
+    outs = [
+        pltpu.make_async_copy(new_keys, keys_hbm, osem.at[0]),
+        pltpu.make_async_copy(new_values, values_hbm, osem.at[1]),
+    ]
+    for copy in outs:
+        copy.start()
 
     rows = 2 * heads
     head_of = iota((rows, LANES), 0) % heads
@@ -118,48 +133,55 @@
     first = iota((rows, LANES), 0) < heads
     tri_row = iota((2 * LANES, 2 * LANES), 0) % LANES
     tri_col = iota((2 * LANES, 2 * LANES), 1)
-    later = jnp.where((tri_row > tri_col) | (tri_col >= LANES), 1.0, 0.0).astype(bf16)
+    later[...] = jnp.where((tri_row > tri_col) | (tri_col >= LANES), 1.0, 0.0).astype(bf16)
     position = iota((rows, LANES), 1)
     zero = jnp.zeros((heads, LANES), f32)
 
-    def one_pair(p, carry):
-        key_copy(p).wait()
-        base = pl.multiple_of(p * rows, rows)
-        both = qrows[pl.ds(base, rows), :]
-        left = jnp.concatenate([both[:heads], zero], axis=0)
-        right = jnp.concatenate([zero, both[heads:]], axis=0)
-        query = jnp.concatenate([left, right], axis=1).astype(bf16)
-        keys = jnp.concatenate([kbuf[2 * p], kbuf[2 * p + 1]], axis=1)
-        scores = dot(query, keys, ((1,), (1,)))
-        limit = jnp.where(first, lengths[2 * p], lengths[2 * p + 1])
-        taken = []
+    def one_group(members):
+        limits = [jnp.where(first, lengths[2 * p], lengths[2 * p + 1]) for p in members]
+        for p in members:
+            key_copy(p).wait()
+        scores = []
+        for p in members:
+            both = qrows[p * rows : (p + 1) * rows, :]
+            left = jnp.concatenate([both[:heads], zero], axis=0)
+            right = jnp.concatenate([zero, both[heads:]], axis=0)
+            query = jnp.concatenate([left, right], axis=1).astype(bf16)
+            keys = jnp.concatenate([kbuf[2 * p], kbuf[2 * p + 1]], axis=1)
+            scores.append(dot(query, keys, ((1,), (1,))))
+        taken = {}
         highs = []
         lows = []
-        for c in range(blocks):
-            z = scores[:, c * LANES : (c + 1) * LANES] * HEAD_DIM ** (-0.5) + offset
-            tail = jnp.log1p(jnp.exp(-jnp.abs(z)))
-            fail = jnp.where(position + c * LANES < limit, -(jnp.maximum(z, 0.0) + tail), 0.0)
-            taken.append(jnp.minimum(z, 0.0) - tail)
-            high, low = split_two(fail)
-            highs.append(high)
-            lows.append(low)
+        for i in range(len(members)):
+            for c in range(blocks):
+                z = scores[i][:, c * LANES : (c + 1) * LANES] * HEAD_DIM ** (-0.5) + offset
+                tail = jnp.log1p(jnp.exp(-jnp.abs(z)))
+                fail = jnp.where(position + c * LANES < limits[i], -(jnp.maximum(z, 0.0) + tail), 0.0)
+                taken[i, c] = jnp.minimum(z, 0.0) - tail
+                high, low = split_two(fail)
+                highs.append(high)
+                lows.append(low)
         halves = jnp.concatenate([jnp.concatenate(highs, axis=0), jnp.concatenate(lows, axis=0)], axis=1)
-        sums = dot(halves, later)
-        carried = jnp.zeros((rows, LANES), f32)
-        sticks = [None] * blocks
-        for c in reversed(range(blocks)):
-            block = sums[c * rows : (c + 1) * rows]
-            share = jnp.exp(taken[c] + (block[:, :LANES] + carried))
-            sticks[c] = jnp.where(position + c * LANES < limit, share, 0.0).astype(bf16)
-            carried = carried + block[:, LANES:]
-        stick = jnp.concatenate(sticks, axis=1)
-        value_copy(p).wait()
-        values = jnp.concatenate([vbuf[2 * p], vbuf[2 * p + 1]], axis=1)
-        attended = dot(stick, values)
-        arows[pl.ds(base, rows), :] = jnp.where(first, attended[:, :LANES], attended[:, LANES:])
-        return carry
-
-    lax.fori_loop(0, pairs, one_pair, 0)
+        sums = dot(halves, later[...])
+        sticks = []
+        for i in range(len(members)):
+            carried = jnp.zeros((rows, LANES), f32)
+            stick = [None] * blocks
+            for c in reversed(range(blocks)):
+                at = (i * blocks + c) * rows
+                share = jnp.exp(taken[i, c] + (sums[at : at + rows, :LANES] + carried))
+                stick[c] = jnp.where(position + c * LANES < limits[i], share, 0.0).astype(bf16)
+                carried = carried + sums[at : at + rows, LANES:]
+            sticks.append(jnp.concatenate(stick, axis=1))
+        for p in members:
+            value_copy(p).wait()
+        for i, p in enumerate(members):
+            values = jnp.concatenate([vbuf[2 * p], vbuf[2 * p + 1]], axis=1)
+            attended = dot(sticks[i], values)
+            arows[p * rows : (p + 1) * rows, :] = jnp.where(first, attended[:, :LANES], attended[:, LANES:])
+
+    for members in groups:
+        one_group(members)
 
     tiles = []
     for q in range(heads // 2):
@@ -174,6 +196,8 @@
     attended = jnp.concatenate(tiles, axis=1).astype(bf16)
     weights[3].wait()
     part_out[...] = dot(attended, wo[...]).astype(bf16)
+    for copy in outs:
+        copy.wait()
 
 
 def attention(lengths, offsets, tokens, gain, key_cache, value_cache, w_query, w_key, w_value, w_out):
@@ -194,7 +218,7 @@
             jax.ShapeDtypeStruct((seqs, kv), bf16),
         ),
         in_specs=[hbm] * 10,
-        out_specs=(vmem, vmem, vmem),
+        out_specs=(vmem, hbm, hbm),
         scratch_shapes=[
             pltpu.SMEM(lengths.shape, jnp.int32),
             pltpu.SMEM(offsets.shape, f32),
@@ -208,11 +232,15 @@
             pltpu.VMEM(w_out.shape, bf16),
             pltpu.VMEM((seqs * heads, LANES), f32),
             pltpu.VMEM((seqs * heads, LANES), f32),
+            pltpu.VMEM((2 * LANES, 2 * LANES), bf16),
+            pltpu.VMEM((seqs, kv), bf16),
+            pltpu.VMEM((seqs, kv), bf16),
             pltpu.SemaphoreType.DMA((8,)),
             pltpu.SemaphoreType.DMA((seqs // 2,)),
             pltpu.SemaphoreType.DMA((seqs // 2,)),
+            pltpu.SemaphoreType.DMA((2,)),
         ],
-        compiler_params=pltpu.CompilerParams(vmem_limit_bytes=32 << 20),
+        compiler_params=pltpu.CompilerParams(vmem_limit_bytes=20 << 20),
         name="attention",
     )(*caches)
 
@@ -256,20 +284,17 @@
         return first, named & (before == slot.astype(f32))
 
     index = iota((seqs, slots), 1)
-    _, chosen = slot_mask(index // capacity, index % capacity)
+    first, chosen = slot_mask(index // capacity, index % capacity)
     rows_out[...] = dot(jnp.where(chosen, 1.0, 0.0).astype(bf16), mine, ((0,), (0,))).astype(bf16)
-    returned = mix_out.shape[1]
-    index = iota((seqs, returned), 1)
-    first, chosen = slot_mask(index // (returned // EXPERTS), index % capacity)
     high, low = split_two(jnp.where(chosen, jnp.where(first, w0, w1), 0.0))
     mix_out[...] = jnp.concatenate([high, low], axis=0)
 
 
-def dispatch(tokens, gain, own, peer, routes, weights, capacity, sources):
+def dispatch(tokens, gain, own, peer, routes, weights, capacity):
     seqs, width = tokens.shape
     vmem = pl.BlockSpec(memory_space=pltpu.VMEM)
     hbm = pl.BlockSpec(memory_space=pltpu.HBM)
-    outs = ((EXPERTS * capacity, width // 2), (seqs, width // 2), (2 * seqs, sources * capacity))
+    outs = ((EXPERTS * capacity, width // 2), (seqs, width // 2), (2 * seqs, EXPERTS * capacity))
     return pl.pallas_call(
         dispatch_kernel,
         out_shape=tuple(jax.ShapeDtypeStruct(shape, bf16) for shape in outs),
@@ -285,33 +310,53 @@
     )(tokens, gain, own, peer, routes, weights)
 
 
-def expert_kernel(own, peer, gate_w, up_w, down_w, keep_out, send_out):
+def own_columns(half):
+    tp_index = lax.axis_index("tp")
+    return pl.multiple_of(tp_index * half, half), pl.multiple_of((1 - tp_index) * half, half)
+
+
+def enter_kernel(own, gate_w, up_w, down_hbm, gate_out, up_out, down_out, sem):
     half = own.shape[1]
-    tp_index = lax.axis_index("tp")
-    mine = pl.multiple_of(tp_index * half, half)
-    other = pl.multiple_of((1 - tp_index) * half, half)
-    x, y = own[...], peer[...]
-
-    def project(w):
-        return dot(x, w[:, pl.ds(mine, half)], ((1,), (1,))) + dot(y, w[:, pl.ds(other, half)], ((1,), (1,)))
-
-    gate = project(gate_w)
-    upward = project(up_w)
+    mine, _ = own_columns(half)
+    copy = pltpu.make_async_copy(down_hbm, down_out, sem)
+    copy.start()
+    gate_out[...] = dot(own[...], gate_w[:, pl.ds(mine, half)], ((1,), (1,)))
+    up_out[...] = dot(own[...], up_w[:, pl.ds(mine, half)], ((1,), (1,)))
+    copy.wait()
+
+
+def hidden_kernel(peer, gate_part, up_part, gate_w, up_w, down_w, hidden_out, send_out):
+    half = peer.shape[1]
+    _, other = own_columns(half)
+    gate = gate_part[...] + dot(peer[...], gate_w[:, pl.ds(other, half)], ((1,), (1,)))
+    upward = up_part[...] + dot(peer[...], up_w[:, pl.ds(other, half)], ((1,), (1,)))
     hidden = (gate / (1.0 + jnp.exp(-gate)) * upward).astype(bf16)
+    hidden_out[...] = hidden
     send_out[...] = dot(hidden, down_w[:, pl.ds(other, half)]).astype(bf16)
-    keep_out[...] = dot(hidden, down_w[:, pl.ds(mine, half)])
-
-
-def expert(own, peer, gate_w, up_w, down_w):
+
+
+def keep_kernel(hidden, down_w, keep_out):
+    half = keep_out.shape[1]
+    mine, _ = own_columns(half)
+    keep_out[...] = dot(hidden[...], down_w[:, pl.ds(mine, half)])
+
+
+def local_call(kernel, outs, *args, far=0):
     vmem = pl.BlockSpec(memory_space=pltpu.VMEM)
+    hbm = pl.BlockSpec(memory_space=pltpu.HBM)
+    rows, half = args[0].shape
+    near = len(args) - far
+    args = args[:near] + tuple(pltpu.with_memory_space_constraint(x, pltpu.HBM) for x in args[near:])
     return pl.pallas_call(
-        expert_kernel,
-        out_shape=(jax.ShapeDtypeStruct(own.shape, f32), jax.ShapeDtypeStruct(own.shape, bf16)),
-        in_specs=[vmem] * 5,
-        out_specs=(vmem, vmem),
-        compiler_params=pltpu.CompilerParams(vmem_limit_bytes=32 << 20),
-        name="expert",
-    )(own, peer, gate_w, up_w, down_w)
+        kernel,
+        out_shape=tuple(jax.ShapeDtypeStruct(shape, kind) for shape, kind in outs),
+        in_specs=[vmem] * near + [hbm] * far,
+        out_specs=(vmem,) * len(outs),
+        scratch_shapes=[pltpu.SemaphoreType.DMA(())] * far,
+        compiler_params=pltpu.CompilerParams(vmem_limit_bytes=12 << 20),
+        cost_estimate=pl.CostEstimate(flops=2 * rows * half * half, transcendentals=0, bytes_accessed=rows * half * 4),
+        name=kernel.__name__[:-7],
+    )(*args)
 
 
 def mix_kernel(mix, returned, middle, out):
@@ -352,7 +397,6 @@
 ):
     seqs, width = tokens.shape
     sources = lax.axis_size("ep")
-    span = sources // EXPERTS
     capacity = 4
     half = width // 2
     swap = [(0, 1), (1, 0)]
@@ -377,19 +421,37 @@
         routes.T,
         route_weights.T,
         capacity,
-        sources,
-    )
-    outgoing = jnp.broadcast_to(
-        rows.reshape(EXPERTS, 1, capacity, half), (EXPERTS, span, capacity, half)
-    ).reshape(sources, capacity, half)
-    arrived = lax.all_to_all(outgoing, "ep", split_axis=0, concat_axis=0, tiled=True)
+    )
+    plane = sources // PLANES
+    sides = EXPERTS // PLANES
+    column_groups = [[p * plane + c for p in range(PLANES)] for c in range(plane)]
+    plane_groups = [[p * plane + c for c in range(plane)] for p in range(PLANES)]
+
+    def exchange(x, groups):
+        return lax.all_to_all(x, "ep", 0, 0, axis_index_groups=groups, tiled=True)
+
+    landed = exchange(rows.reshape(PLANES, sides * capacity, half), column_groups)
+    landed = landed.reshape(PLANES, sides, capacity, half).transpose(1, 0, 2, 3)
+    outgoing = jnp.broadcast_to(landed[:, None], (sides, plane // sides) + landed.shape[1:])
+    arrived = exchange(outgoing.reshape((plane,) + landed.shape[1:]), plane_groups)
     own = arrived.reshape(sources * capacity, half)
     peer = lax.ppermute(own, "tp", swap)
-    keep, send = expert(own, peer, w_gate.T, w_up.T, w_down)
+    gate_w, up_w = w_gate.T, w_up.T
+    inner = (own.shape[0], gate_w.shape[0])
+    *parts, down_w = local_call(
+        enter_kernel, ((inner, f32), (inner, f32), (w_down.shape, bf16)), own, gate_w, up_w, w_down, far=1
+    )
+    hidden, send = local_call(
+        hidden_kernel, ((inner, bf16), (own.shape, bf16)), peer, *parts, gate_w, up_w, down_w
+    )
     got = lax.ppermute(send, "tp", swap)
-    shares = (keep + got.astype(f32)).astype(bf16).reshape(sources, capacity, half)
-    returned = lax.all_to_all(shares, "ep", split_axis=0, concat_axis=0, tiled=True)
-    layer_out = mix_rows(mix, returned.reshape(sources * capacity, half), middle)
+    (keep,) = local_call(keep_kernel, ((own.shape, f32),), hidden, down_w)
+    shares = (keep + got.astype(f32)).astype(bf16).reshape(plane, PLANES, capacity, half)
+    landed = exchange(shares, plane_groups)
+    landed = landed.reshape(sides, plane // sides, PLANES, capacity, half).astype(f32).sum(axis=1)
+    landed = landed.astype(bf16).transpose(1, 0, 2, 3).reshape(PLANES, sides * capacity, half)
+    returned = exchange(landed, column_groups)
+    layer_out = mix_rows(mix, returned.reshape(EXPERTS * capacity, half), middle)
     return (layer_out, new_keys, new_values)
 
 

time: 83.4 us -> 74.8 us (0.90)
  blocking collectives: 57.2 us -> 52.8 us
  Pallas kernels: 12.9 us -> 10.6 us
  waiting for transfers between devices: 3.93 us -> 2.3 us
  local copies, waits for them, and re-layouts: 1.6 us -> 0.56 us
    all_to_all x2 -> x4, blocking collectives: 57.2 us -> 52.8 us  [exchange(): return lax.all_to_all(x, 'ep', 0, 0, axis_index_groups=groups, tiled=True)]
    pallas_call x1, Pallas kernels: 9.61 us -> 6.6 us  [attention(): pl.pallas_call(attention_kernel, out_shape=(jax.ShapeDtypeStruct((seqs, w...]
    ppermute x1, waiting for transfers between devices: 1.54 us -> 0.34 us  [shards(): peer = lax.ppermute(own, 'tp', swap)]
    reshape x1, local copies, waits for them, and re-layouts: 1.16 us -> 0.12 us  [shards(): own = arrived.reshape(sources * capacity, half)]
    pallas_call x1 -> x3, Pallas kernels: 1.88 us -> 2.76 us  [local_call(): pl.pallas_call(kernel, out_shape=tuple((jax.ShapeDtypeStruct(shape, kind)...]
  transfers between devices with their start and end apart: 3 -> 3, of which waited for: 3 -> 3; matrix products, arithmetic and copies ran while one was open for 0% -> 0% of each run, Pallas kernels for 0% -> 2%
where the time goes in v2:
time: 74.8 us; the launch traced here: 74.2 us
  blocking collectives  52.8 us (71%)
  Pallas kernels  10.6 us (14%)
  starting transfers between devices  6.73 us (9%)
  waiting for transfers between devices  2.3 us (3%)
  between operations  0.77 us (1%)
    all_to_all x4, blocking collectives, exchange(): return lax.all_to_all(x, 'ep', 0, 0, axis_index_groups=groups, tiled=True)  52.8 us
    pallas_call x1, Pallas kernels, attention(): pl.pallas_call(attention_kernel, out_shape=(jax.ShapeDtypeStruct((seqs, w...  6.6 us
    ppermute x1, starting transfers between devices, shards(): other_part = lax.ppermute(part, 'tp', swap)  3.29 us
    ppermute x1, starting transfers between devices, shards(): peer = lax.ppermute(own, 'tp', swap)  2.97 us
    pallas_call x3, Pallas kernels, local_call(): pl.pallas_call(kernel, out_shape=tuple((jax.ShapeDtypeStruct(shape, kind)...  2.76 us
  transfers between devices with their start and end apart: 3, of which 3 were waited for; matrix products, arithmetic and copies ran while one was open for 0% of the time, Pallas kernels for 2%

profile of v2, /device:TPU:1, one launch (start us, length us, event | category | flops | bytes accessed | tf_op | source)
XLA Modules:
  0.0 74.2 jit_solution(1263127754623254826)
XLA Ops:
  0.6 0.0 copy-start.2
  0.6 0.0 copy-start.3
  0.7 0.0 copy-start.4
  0.7 0.0 copy-start.5
  0.7 0.0 copy-start
  0.7 0.0 copy-start.1
  0.7 6.6 %attention.1 = (bf16[16,1024]{1,0:T(8,128)(2,1)S(1)}, bf16[16,128]{1,0:T(8,128)(2,1)}, bf16[16,128]{1,0:T(8,128)(2,1)}) custom-call(s32[16]{0:T(128)} %lengths_hbm.1, f32[8]{0:T(128)} %offsets_hbm.1, bf16[16,1024]{1,0:T(8,128)(2,1)} %tokens.1, f32[1,1024]{1,0:T(1,128)} %bitcast.27, bf16[16,1024,128]{2,1,0:T(8,128)(2,1)} %key_hbm.1, ...), custom_call_target="tpu_custom_call" | custom-call | tf_op jit(solution)/shard_map/attention/pallas_call | solution.py:213
  7.3 3.3 %collective-permute-start = (bf16[16,1024]{1,0:T(8,128)(2,1)S(1)}, bf16[16,1024]{1,0:T(8,128)(2,1)S(1)}, u32[]{:S(2)}, u32[]{:S(2)}) collective-permute-start(bf16[16,1024]{1,0:T(8,128)(2,1)S(1)} %get-tuple-element.14.own), channel_id=1, source_target_pairs={{0,1},{1,0},{2,3},{3,2},{4,5},{5,4},{6,7},{7,6},{8,9},{9,8},{10,11... | collective-permute-start | bytes 98312 | tf_op jit(solution)/shard_map/ppermute | solution.py:415
  10.6 0.9 %collective-permute-done.peer = bf16[16,1024]{1,0:T(8,128)(2,1)S(1)} collective-permute-done((bf16[16,1024]{1,0:T(8,128)(2,1)S(1)}, bf16[16,1024]{1,0:T(8,128)(2,1)S(1)}, u32[]{:S(2)}, u32[]{:S(2)}) %collective-permute-start) | collective-permute-done | bytes 32800 | tf_op jit(solution)/shard_map/ppermute | solution.py:415
  11.5 0.0 copy-done.2
  11.5 0.0 copy-done.3
  11.5 0.0 copy-done.4
  11.5 0.0 copy-done.5
  11.5 0.5 dispatch.1
  12.0 13.5 %all_to_all.20 = bf16[8,8,512]{2,1,0:T(8,128)(2,1)S(1)} all-to-all(bf16[8,8,512]{2,1,0:T(8,128)(2,1)S(1)} %bitcast.19), channel_id=1, replica_groups={{0,32,64,96,128,160,192,224},{2,34,66,98,130,162,194,226},{4,36,68,100,..., dimensions={0} | all-to-all | bytes 131072 | tf_op jit(solution)/shard_map/all_to_all | solution.py:431
  25.6 0.2 broadcast_in_dim.2
  25.8 16.2 %all_to_all.21 = bf16[16,8,4,512]{3,2,1,0:T(4,128)(2,1)S(1)} all-to-all(bf16[16,8,4,512]{3,2,1,0:T(4,128)(2,1)S(1)} %bitcast.23), channel_id=1, replica_groups={{0,2,4,6,8,10,12,14,16,18,20,22,24,26,28,30},{32,34,36,38,40,42,44,46,4..., dimensions={0} | all-to-all | bytes 1048576 | tf_op jit(solution)/shard_map/all_to_all | solution.py:431
  42.0 0.1 reshape.42.own
  42.1 3.0 %collective-permute-start.1 = (bf16[512,512]{1,0:T(8,128)(2,1)S(1)}, bf16[512,512]{1,0:T(8,128)(2,1)S(1)}, u32[]{:S(2)}, u32[]{:S(2)}) collective-permute-start(bf16[512,512]{1,0:T(8,128)(2,1)S(1)} %reshape.42.own), channel_id=1, source_target_pairs={{0,1},{1,0},{2,3},{3,2},{4,5},{5,4},{6,7},{7,6},{8,9},{9,8},{10,11... | collective-permute-start | bytes 1572872 | tf_op jit(solution)/shard_map/ppermute | solution.py:438
  45.1 0.0 copy-done
  45.1 1.2 %enter.1 = (f32[512,448]{1,0:T(8,128)S(1)}, f32[512,448]{1,0:T(8,128)S(1)}, bf16[448,1024]{1,0:T(8,128)(2,1)S(1)}) custom-call(bf16[512,512]{1,0:T(8,128)(2,1)S(1)} %reshape.42.own, bf16[448,1024]{1,0:T(8,128)(2,1)S(1)} %bitcast.14, bf16[448,1024]{1,0:T(8,128)(2,1)S(1)} %bitcast.16, bf16[448,1024]{1,0:T(8,128)(2,1)} %down_hbm.1), custom_call_target="tpu_custom_call" | custom-call | flops 268435456 | bytes 1048576 | tf_op jit(solution)/shard_map/enter/pallas_call | solution.py:350
  46.3 0.3 collective-permute-done.1.peer
  46.6 1.1 %hidden.1 = (bf16[512,448]{1,0:T(8,128)(2,1)S(1)}, bf16[512,512]{1,0:T(8,128)(2,1)S(1)}) custom-call(bf16[512,512]{1,0:T(8,128)(2,1)S(1)} %collective-permute-done.1.peer, f32[512,448]{1,0:T(8,128)S(1)} %get-tuple-element.17.gate_part, f32[512,448]{1,0:T(8,128)S(1)} %get-tuple-element.18.up_part, bf16[448,1024]{1,0:T(8,128)(2,1)S(1)} %bitcast.15, ...), custom_call_target="tpu_custom_call" | custom-call | flops 268435456 | bytes 1048576 | tf_op jit(solution)/shard_map/hidden/pallas_call | solution.py:350
  47.8 0.5 collective-permute-start.2
  48.2 0.4 keep.1
  48.7 1.1 %collective-permute-done.2 = bf16[512,512]{1,0:T(8,128)(2,1)S(1)} collective-permute-done((bf16[512,512]{1,0:T(8,128)(2,1)S(1)}, bf16[512,512]{1,0:T(8,128)(2,1)S(1)}, u32[]{:S(2)}, u32[]{:S(2)}) %collective-permute-start.2) | collective-permute-done | bytes 524320 | tf_op jit(solution)/shard_map/ppermute | solution.py:447
  49.8 0.2 add_convert_fusion
  49.9 0.1 reshape.43
  50.1 13.4 %all_to_all.22 = bf16[16,8,4,512]{3,2,1,0:T(4,128)(2,1)S(1)} all-to-all(bf16[16,8,4,512]{3,2,1,0:T(4,128)(2,1)S(1)} %reshape.43), channel_id=1, replica_groups={{0,2,4,6,8,10,12,14,16,18,20,22,24,26,28,30},{32,34,36,38,40,42,44,46,4..., dimensions={0} | all-to-all | bytes 1048576 | tf_op jit(solution)/shard_map/all_to_all | solution.py:431
  63.4 0.2 bitcast_reduce_fusion
  63.7 9.7 %all_to_all.23 = bf16[8,8,512]{2,1,0:T(8,128)(2,1)S(1)} all-to-all(bf16[8,8,512]{2,1,0:T(8,128)(2,1)S(1)} %copy.26), channel_id=1, replica_groups={{0,32,64,96,128,160,192,224},{2,34,66,98,130,162,194,226},{4,36,68,100,..., dimensions={0} | all-to-all | bytes 131072 | tf_op jit(solution)/shard_map/all_to_all | solution.py:431
  73.4 0.7 mix.1
  (5 shorter events, 0.1 us)
Async XLA Ops:
  0.6 10.8 %copy-start.2 = (bf16[16,1024]{1,0:T(8,128)(2,1)S(1)}, bf16[16,1024]{1,0:T(8,128)(2,1)}, u32[]{:S(2)}) copy-start(bf16[16,1024]{1,0:T(8,128)(2,1)} %tokens.1) | copy-start | bytes 98308
  0.6 10.8 %copy-start.3 = (s32[2048,2]{0,1:T(2,128)S(1)}, s32[2048,2]{0,1:T(2,128)}, u32[]{:S(2)}) copy-start(s32[2048,2]{0,1:T(2,128)} %param.18) | copy-start | bytes 49156
  0.7 10.8 %copy-start.4 = (f32[2048,2]{0,1:T(2,128)S(1)}, f32[2048,2]{0,1:T(2,128)}, u32[]{:S(2)}) copy-start(f32[2048,2]{0,1:T(2,128)} %param.19) | copy-start | bytes 49156
  0.7 10.8 %copy-start.5 = (f32[1024]{0:T(1024)S(1)}, f32[1024]{0:T(1024)}, u32[]{:S(2)}) copy-start(f32[1024]{0:T(1024)} %param.28) | copy-start | bytes 12292
  0.7 44.4 %copy-start = (bf16[1024,448]{0,1:T(8,128)(2,1)S(1)}, bf16[1024,448]{0,1:T(8,128)(2,1)}, u32[]{:S(2)}) copy-start(bf16[1024,448]{0,1:T(8,128)(2,1)} %param.29) | copy-start | bytes 2752516
  0.7 44.4 %copy-start.1 = (bf16[1024,448]{0,1:T(8,128)(2,1)S(1)}, bf16[1024,448]{0,1:T(8,128)(2,1)}, u32[]{:S(2)}) copy-start(bf16[1024,448]{0,1:T(8,128)(2,1)} %param.30) | copy-start | bytes 2752516
  7.3 4.1 %collective-permute-start = (bf16[16,1024]{1,0:T(8,128)(2,1)S(1)}, bf16[16,1024]{1,0:T(8,128)(2,1)S(1)}, u32[]{:S(2)}, u32[]{:S(2)}) collective-permute-start(bf16[16,1024]{1,0:T(8,128)(2,1)S(1)} %get-tuple-element.14.own), channel_id=1, source_target_pairs={{0,1},{1,0},{2,3},{3,2},{4,5},{5,4},{6,7},{7,6},{8,9},{9,8},{10,11... | collective-permute-start | bytes 98312 | tf_op jit(solution)/shard_map/ppermute | solution.py:415
  42.1 4.5 %collective-permute-start.1 = (bf16[512,512]{1,0:T(8,128)(2,1)S(1)}, bf16[512,512]{1,0:T(8,128)(2,1)S(1)}, u32[]{:S(2)}, u32[]{:S(2)}) collective-permute-start(bf16[512,512]{1,0:T(8,128)(2,1)S(1)} %reshape.42.own), channel_id=1, source_target_pairs={{0,1},{1,0},{2,3},{3,2},{4,5},{5,4},{6,7},{7,6},{8,9},{9,8},{10,11... | collective-permute-start | bytes 1572872 | tf_op jit(solution)/shard_map/ppermute | solution.py:438
  47.8 2.0 %collective-permute-start.2 = (bf16[512,512]{1,0:T(8,128)(2,1)S(1)}, bf16[512,512]{1,0:T(8,128)(2,1)S(1)}, u32[]{:S(2)}, u32[]{:S(2)}) collective-permute-start(bf16[512,512]{1,0:T(8,128)(2,1)S(1)} %get-tuple-element.21), channel_id=1, source_target_pairs={{0,1},{1,0},{2,3},{3,2},{4,5},{5,4},{6,7},{7,6},{8,9},{9,8},{10,11... | collective-permute-start | bytes 1572872 | tf_op jit(solution)/shard_map/ppermute | solution.py:447

commit v3 on v2

--- a/solution.py
+++ b/solution.py
@@ -3,6 +3,7 @@
 from jax import lax
 from jax.experimental import pallas as pl
 from jax.experimental.pallas import tpu as pltpu
+from jax.sharding import Mesh
 from jax.sharding import PartitionSpec as P
 
 HEAD_DIM = 64
@@ -10,6 +11,7 @@
 LANES = 128
 GROUPS = (4, 4)
 PLANES = 8
+SIDES = EXPERTS // PLANES
 norm_eps = 1e-06
 
 f32 = jnp.float32
@@ -69,9 +71,8 @@
     vsem,
     osem,
 ):
-    seqs, context, width = kbuf.shape
+    seqs, context, _ = kbuf.shape
     heads = qrows.shape[0] // seqs
-    pairs = seqs // 2
     blocks = context // LANES
 
     def key_copy(p):
@@ -200,16 +201,14 @@
         copy.wait()
 
 
-def attention(lengths, offsets, tokens, gain, key_cache, value_cache, w_query, w_key, w_value, w_out):
+def attention(*args):
+    caches = [pltpu.with_memory_space_constraint(x, pltpu.HBM) for x in args]
+    lengths, offsets, tokens, gain, key_cache, value_cache, w_query, w_key, w_value, w_out = args
     seqs, width = tokens.shape
     heads = offsets.shape[0]
     kv = w_key.shape[1]
     vmem = pl.BlockSpec(memory_space=pltpu.VMEM)
     hbm = pl.BlockSpec(memory_space=pltpu.HBM)
-    caches = [
-        pltpu.with_memory_space_constraint(x, pltpu.HBM)
-        for x in (lengths, offsets, tokens, gain, key_cache, value_cache, w_query, w_key, w_value, w_out)
-    ]
     return pl.pallas_call(
         attention_kernel,
         out_shape=(
@@ -217,7 +216,7 @@
             jax.ShapeDtypeStruct((seqs, kv), bf16),
             jax.ShapeDtypeStruct((seqs, kv), bf16),
         ),
-        in_specs=[hbm] * 10,
+        in_specs=[hbm] * len(args),
         out_specs=(vmem, hbm, hbm),
         scratch_shapes=[
             pltpu.SMEM(lengths.shape, jnp.int32),
@@ -249,9 +248,9 @@
     tokens, gain, own, peer, routes_hbm, weights_hbm, rows_out, middle_out, mix_out, route, weight, sems
 ):
     seqs, width = tokens.shape
-    slots, half = rows_out.shape
-    capacity = slots // EXPERTS
-    start = lax.axis_index("ep") * seqs
+    half = width // 2
+    own_slots = rows_out.shape[0] // EXPERTS
+    start = (lax.axis_index("plane") * lax.axis_size("spot") + lax.axis_index("spot")) * seqs
     tile = pl.multiple_of(start // LANES * LANES, LANES)
     copies = [
         pltpu.make_async_copy(routes_hbm.at[:, pl.ds(tile, LANES)], route, sems.at[0]),
@@ -259,10 +258,10 @@
     ]
     for copy in copies:
         copy.start()
-    low_half = lax.axis_index("tp") == 0
+    tp_index = lax.axis_index("tp")
+    low_half = tp_index == 0
     middle = (tokens[...].astype(f32) + own[...].astype(f32) + peer[...].astype(f32)).astype(bf16)
-    moe_in = rms_rows(middle, gain[...]).astype(f32)
-    mine = jnp.where(low_half, moe_in[:, :half], moe_in[:, half:]).astype(bf16)
+    moe_in = rms_rows(middle, gain[...])
     middle = middle.astype(f32)
     middle_out[...] = jnp.where(low_half, middle[:, :half], middle[:, half:]).astype(bf16)
     for copy in copies:
@@ -283,9 +282,13 @@
         before = dot(earlier, jnp.where(named, 1.0, 0.0).astype(bf16))
         return first, named & (before == slot.astype(f32))
 
-    index = iota((seqs, slots), 1)
-    first, chosen = slot_mask(index // capacity, index % capacity)
-    rows_out[...] = dot(jnp.where(chosen, 1.0, 0.0).astype(bf16), mine, ((0,), (0,))).astype(bf16)
+    index = iota((seqs, rows_out.shape[0]), 1)
+    _, chosen = slot_mask(index // own_slots, tp_index * own_slots + index % own_slots)
+    rows_out[...] = dot(jnp.where(chosen, 1.0, 0.0).astype(bf16), moe_in, ((0,), (0,))).astype(bf16)
+    index = iota((seqs, mix_out.shape[1]), 1)
+    source, part = index // (SIDES * own_slots), index // own_slots
+    expert = source // 2 * SIDES + part % SIDES
+    first, chosen = slot_mask(expert, source % 2 * own_slots + index % own_slots)
     high, low = split_two(jnp.where(chosen, jnp.where(first, w0, w1), 0.0))
     mix_out[...] = jnp.concatenate([high, low], axis=0)
 
@@ -294,7 +297,7 @@
     seqs, width = tokens.shape
     vmem = pl.BlockSpec(memory_space=pltpu.VMEM)
     hbm = pl.BlockSpec(memory_space=pltpu.HBM)
-    outs = ((EXPERTS * capacity, width // 2), (seqs, width // 2), (2 * seqs, EXPERTS * capacity))
+    outs = ((EXPERTS * capacity // 2, width), (seqs, width // 2), (2 * seqs, EXPERTS * capacity))
     return pl.pallas_call(
         dispatch_kernel,
         out_shape=tuple(jax.ShapeDtypeStruct(shape, bf16) for shape in outs),
@@ -310,53 +313,41 @@
     )(tokens, gain, own, peer, routes, weights)
 
 
-def own_columns(half):
-    tp_index = lax.axis_index("tp")
-    return pl.multiple_of(tp_index * half, half), pl.multiple_of((1 - tp_index) * half, half)
-
-
-def enter_kernel(own, gate_w, up_w, down_hbm, gate_out, up_out, down_out, sem):
-    half = own.shape[1]
-    mine, _ = own_columns(half)
-    copy = pltpu.make_async_copy(down_hbm, down_out, sem)
-    copy.start()
-    gate_out[...] = dot(own[...], gate_w[:, pl.ds(mine, half)], ((1,), (1,)))
-    up_out[...] = dot(own[...], up_w[:, pl.ds(mine, half)], ((1,), (1,)))
-    copy.wait()
-
-
-def hidden_kernel(peer, gate_part, up_part, gate_w, up_w, down_w, hidden_out, send_out):
-    half = peer.shape[1]
-    _, other = own_columns(half)
-    gate = gate_part[...] + dot(peer[...], gate_w[:, pl.ds(other, half)], ((1,), (1,)))
-    upward = up_part[...] + dot(peer[...], up_w[:, pl.ds(other, half)], ((1,), (1,)))
-    hidden = (gate / (1.0 + jnp.exp(-gate)) * upward).astype(bf16)
-    hidden_out[...] = hidden
-    send_out[...] = dot(hidden, down_w[:, pl.ds(other, half)]).astype(bf16)
-
-
-def keep_kernel(hidden, down_w, keep_out):
-    half = keep_out.shape[1]
-    mine, _ = own_columns(half)
-    keep_out[...] = dot(hidden[...], down_w[:, pl.ds(mine, half)])
-
-
-def local_call(kernel, outs, *args, far=0):
+def expert_kernel(rows, gate_own, up_own, down_own, gate_hbm, up_hbm, down_hbm, out, gate_peer, up_peer, down_peer, sems):
+    peers = ((gate_hbm, gate_peer), (up_hbm, up_peer), (down_hbm, down_peer))
+    copies = [pltpu.make_async_copy(src, dst, sems.at[i]) for i, (src, dst) in enumerate(peers)]
+    for copy in copies:
+        copy.start()
+    x = rows[...]
+
+    def hidden_of(gate, upward):
+        return (gate / (1.0 + jnp.exp(-gate)) * upward).astype(bf16)
+
+    def project(w):
+        return dot(x, w, ((1,), (1,)))
+
+    total = dot(hidden_of(project(gate_own[...]), project(up_own[...])), down_own[...])
+    copies[0].wait()
+    gate = project(gate_peer[...])
+    copies[1].wait()
+    hidden = hidden_of(gate, project(up_peer[...]))
+    copies[2].wait()
+    out[...] = (total + dot(hidden, down_peer[...])).astype(bf16)
+
+
+def expert(rows, own, peers):
     vmem = pl.BlockSpec(memory_space=pltpu.VMEM)
     hbm = pl.BlockSpec(memory_space=pltpu.HBM)
-    rows, half = args[0].shape
-    near = len(args) - far
-    args = args[:near] + tuple(pltpu.with_memory_space_constraint(x, pltpu.HBM) for x in args[near:])
+    peers = [pltpu.with_memory_space_constraint(w, pltpu.HBM) for w in peers]
     return pl.pallas_call(
-        kernel,
-        out_shape=tuple(jax.ShapeDtypeStruct(shape, kind) for shape, kind in outs),
-        in_specs=[vmem] * near + [hbm] * far,
-        out_specs=(vmem,) * len(outs),
-        scratch_shapes=[pltpu.SemaphoreType.DMA(())] * far,
-        compiler_params=pltpu.CompilerParams(vmem_limit_bytes=12 << 20),
-        cost_estimate=pl.CostEstimate(flops=2 * rows * half * half, transcendentals=0, bytes_accessed=rows * half * 4),
-        name=kernel.__name__[:-7],
-    )(*args)
+        expert_kernel,
+        out_shape=jax.ShapeDtypeStruct(rows.shape, bf16),
+        in_specs=[vmem] * 4 + [hbm] * 3,
+        out_specs=vmem,
+        scratch_shapes=[pltpu.VMEM(w.shape, bf16) for w in peers] + [pltpu.SemaphoreType.DMA((3,))],
+        compiler_params=pltpu.CompilerParams(vmem_limit_bytes=16 << 20),
+        name="expert",
+    )(rows, *own, *peers)
 
 
 def mix_kernel(mix, returned, middle, out):
@@ -395,11 +386,19 @@
     w_up,
     w_down,
 ):
-    seqs, width = tokens.shape
-    sources = lax.axis_size("ep")
+    _, width = tokens.shape
+    planes, plane = lax.axis_size("plane"), lax.axis_size("spot")
     capacity = 4
     half = width // 2
     swap = [(0, 1), (1, 0)]
+
+    def named_swap(x):
+        return lax.ppermute(x, "tp", swap)
+
+    def exchange(x, axes):
+        return lax.all_to_all(x, axes, 0, 0, tiled=True)
+
+    gate_w, up_w = w_gate.T, w_up.T
     part, new_keys, new_values = attention(
         lengths,
         score_offset,
@@ -412,7 +411,7 @@
         w_value,
         w_out,
     )
-    other_part = lax.ppermute(part, "tp", swap)
+    other_part = named_swap(part)
     rows, middle, mix = dispatch(
         tokens,
         ffn_gain.reshape(1, width),
@@ -422,47 +421,35 @@
         route_weights.T,
         capacity,
     )
-    plane = sources // PLANES
-    sides = EXPERTS // PLANES
-    column_groups = [[p * plane + c for p in range(PLANES)] for c in range(plane)]
-    plane_groups = [[p * plane + c for c in range(plane)] for p in range(PLANES)]
-
-    def exchange(x, groups):
-        return lax.all_to_all(x, "ep", 0, 0, axis_index_groups=groups, tiled=True)
-
-    landed = exchange(rows.reshape(PLANES, sides * capacity, half), column_groups)
-    landed = landed.reshape(PLANES, sides, capacity, half).transpose(1, 0, 2, 3)
-    outgoing = jnp.broadcast_to(landed[:, None], (sides, plane // sides) + landed.shape[1:])
-    arrived = exchange(outgoing.reshape((plane,) + landed.shape[1:]), plane_groups)
-    own = arrived.reshape(sources * capacity, half)
-    peer = lax.ppermute(own, "tp", swap)
-    gate_w, up_w = w_gate.T, w_up.T
-    inner = (own.shape[0], gate_w.shape[0])
-    *parts, down_w = local_call(
-        enter_kernel, ((inner, f32), (inner, f32), (w_down.shape, bf16)), own, gate_w, up_w, w_down, far=1
-    )
-    hidden, send = local_call(
-        hidden_kernel, ((inner, bf16), (own.shape, bf16)), peer, *parts, gate_w, up_w, down_w
-    )
-    got = lax.ppermute(send, "tp", swap)
-    (keep,) = local_call(keep_kernel, ((own.shape, f32),), hidden, down_w)
-    shares = (keep + got.astype(f32)).astype(bf16).reshape(plane, PLANES, capacity, half)
-    landed = exchange(shares, plane_groups)
-    landed = landed.reshape(sides, plane // sides, PLANES, capacity, half).astype(f32).sum(axis=1)
-    landed = landed.astype(bf16).transpose(1, 0, 2, 3).reshape(PLANES, sides * capacity, half)
-    returned = exchange(landed, column_groups)
+    own_weights = (gate_w, up_w, w_down)
+    *waiting, part = lax.optimization_barrier(own_weights + (part,))
+    peer_weights = [named_swap(w) for w in waiting]
+    slots = capacity // 2
+    landed = exchange(rows.reshape(planes, SIDES * slots, width), "plane")
+    landed = landed.reshape(planes, SIDES, slots, width).transpose(1, 0, 2, 3)
+    landed = landed.reshape(SIDES, 1, planes * slots, width)
+    outgoing = jnp.broadcast_to(landed, (SIDES, plane // SIDES, planes * slots, width))
+    arrived = exchange(outgoing.reshape(plane, planes * slots, width), "spot")
+    shares = expert(arrived.reshape(plane * planes * slots, width), own_weights, peer_weights)
+    landed = exchange(shares.reshape(plane, planes * slots, width), "spot")
+    landed = landed.reshape(SIDES, plane // SIDES, planes * slots, width).astype(f32).sum(axis=1).astype(bf16)
+    landed = landed.reshape(SIDES, planes, slots, 2, half).transpose(1, 3, 0, 2, 4)
+    returned = exchange(landed.reshape(2 * planes, SIDES * slots, half), ("plane", "tp"))
     layer_out = mix_rows(mix, returned.reshape(EXPERTS * capacity, half), middle)
     return (layer_out, new_keys, new_values)
 
 
 def solution(mesh):
+    devices = mesh.devices
+    fine = Mesh(devices.reshape(PLANES, -1, devices.shape[-1]), ("plane", "spot", "tp"))
+    ep = ("plane", "spot")
     in_specs = (
-        P("ep", None),
-        P("ep"),
+        P(ep, None),
+        P(ep),
         P(),
         P(),
-        P("ep", None, "tp"),
-        P("ep", None, "tp"),
+        P(ep, None, "tp"),
+        P(ep, None, "tp"),
         P(None, "tp"),
         P(None, "tp"),
         P(None, "tp"),
@@ -470,9 +457,9 @@
         P("tp"),
         P(),
         P(),
-        P(None, ("ep", "tp")),
-        P(None, ("ep", "tp")),
-        P(("ep", "tp"), None),
+        P(None, ep + ("tp",)),
+        P(None, ep + ("tp",)),
+        P(ep + ("tp",), None),
     )
-    out_specs = (P("ep", "tp"), P("ep", "tp"), P("ep", "tp"))
-    return jax.shard_map(shards, mesh=mesh, in_specs=in_specs, out_specs=out_specs, check_vma=False)
+    out_specs = (P(ep, "tp"), P(ep, "tp"), P(ep, "tp"))
+    return jax.shard_map(shards, mesh=fine, in_specs=in_specs, out_specs=out_specs, check_vma=False)

time: 74.8 us -> 77 us (1.029)
  blocking collectives: 52.8 us -> 55.9 us
  starting transfers between devices: 6.73 us -> 3.91 us
  waiting for transfers between devices: 2.3 us -> 4.24 us
  Pallas kernels: 10.6 us -> 11.5 us
    all_to_all x4, blocking collectives: 52.8 us -> 55.9 us  [exchange(): return lax.all_to_all(x, axes, 0, 0, tiled=True)]
    ppermute x3 -> x4, starting transfers between devices: 6.73 us -> 3.91 us  [named_swap(): return lax.ppermute(x, 'tp', swap)]
    ppermute x3 -> x4, waiting for transfers between devices: 2.3 us -> 4.24 us  [named_swap(): return lax.ppermute(x, 'tp', swap)]
    pallas_call x3 -> x1, Pallas kernels: 2.76 us -> 3.38 us  [expert(): pl.pallas_call(expert_kernel, out_shape=jax.ShapeDtypeStruct(rows.shape,...]
  transfers between devices with their start and end apart: 3 -> 4, of which waited for: 3 -> 1; matrix products, arithmetic and copies ran while one was open for 0% -> 0% of each run, Pallas kernels for 2% -> 1%
where the time goes in v3:
time: 77 us; the launch traced here: 76.8 us
  blocking collectives  55.9 us (73%)
  Pallas kernels  11.5 us (15%)
  waiting for transfers between devices  4.24 us (6%)
  starting transfers between devices  3.91 us (5%)
  between operations  0.79 us (1%)
    all_to_all x4, blocking collectives, exchange(): return lax.all_to_all(x, axes, 0, 0, tiled=True)  55.9 us
    pallas_call x1, Pallas kernels, attention(): pl.pallas_call(attention_kernel, out_shape=(jax.ShapeDtypeStruct((seqs, w...  6.85 us
    ppermute x4, waiting for transfers between devices, named_swap(): return lax.ppermute(x, 'tp', swap)  4.24 us
    ppermute x4, starting transfers between devices, named_swap(): return lax.ppermute(x, 'tp', swap)  3.91 us
    pallas_call x1, Pallas kernels, expert(): pl.pallas_call(expert_kernel, out_shape=jax.ShapeDtypeStruct(rows.shape,...  3.38 us
  transfers between devices with their start and end apart: 4, of which 1 were waited for; matrix products, arithmetic and copies ran while one was open for 0% of the time, Pallas kernels for 1%

profile of v3, /device:TPU:1, one launch (start us, length us, event | category | flops | bytes accessed | tf_op | source)
XLA Modules:
  0.0 76.8 jit_solution(3973746628682956289)
XLA Ops:
  0.6 0.0 copy-start
  0.6 0.0 copy-start.1
  0.7 0.0 copy-start.2
  0.7 0.0 copy-start.3
  0.7 0.0 copy-start.4
  0.7 0.0 copy-start.5
  0.7 0.0 copy-start.6
  0.7 6.9 %attention.1 = (bf16[16,1024]{1,0:T(8,128)(2,1)S(1)}, bf16[16,128]{1,0:T(8,128)(2,1)}, bf16[16,128]{1,0:T(8,128)(2,1)}) custom-call(s32[16]{0:T(128)} %lengths_hbm.1, f32[8]{0:T(128)} %offsets_hbm.1, bf16[16,1024]{1,0:T(8,128)(2,1)} %tokens.1, f32[1,1024]{1,0:T(1,128)} %bitcast.29, bf16[16,1024,128]{2,1,0:T(8,128)(2,1)} %key_hbm.1, ...), custom_call_target="tpu_custom_call" | custom-call | tf_op jit(solution)/shard_map/attention/pallas_call | solution.py:212
  7.6 0.0 copy-done
  7.6 3.3 %collective-permute-start.1 = (bf16[448,1024]{1,0:T(8,128)(2,1)S(1)}, bf16[448,1024]{1,0:T(8,128)(2,1)}, u32[]{:S(2)}, u32[]{:S(2)}) collective-permute-start(bf16[448,1024]{1,0:T(8,128)(2,1)S(1)} %bitcast.18), channel_id=1, source_target_pairs={{0,1},{1,0},{2,3},{3,2},{4,5},{5,4},{6,7},{7,6},{8,9},{9,8},{10,11... | collective-permute-start | bytes 2752520 | tf_op jit(solution)/shard_map/ppermute | solution.py:396
  10.9 0.0 copy-done.1
  10.9 0.1 collective-permute-start.2
  11.0 0.0 copy-done.2
  11.0 0.4 collective-permute-start.3
  11.4 0.1 collective-permute-start
  11.5 4.2 %collective-permute-done.peer = bf16[16,1024]{1,0:T(8,128)(2,1)S(1)} collective-permute-done((bf16[16,1024]{1,0:T(8,128)(2,1)S(1)}, bf16[16,1024]{1,0:T(8,128)(2,1)S(1)}, u32[]{:S(2)}, u32[]{:S(2)}) %collective-permute-start) | collective-permute-done | bytes 32800 | tf_op jit(solution)/shard_map/ppermute | solution.py:396
  15.7 0.0 copy-done.3
  15.7 0.0 copy-done.4
  15.7 0.6 dispatch.1
  16.3 13.5 %all_to_all.20 = bf16[8,4,1024]{2,1,0:T(4,128)(2,1)S(1)} all-to-all(bf16[8,4,1024]{2,1,0:T(4,128)(2,1)S(1)} %reshape.43), channel_id=1, replica_groups=mesh['plane'=8,'spot'=16,'tp'=2] {'plane'}, dimensions={0} | all-to-all | bytes 131072 | tf_op jit(solution)/shard_map/all_to_all | solution.py:399
  29.9 0.1 copy.26
  30.0 0.1 broadcast_in_dim.8
  30.0 16.2 %all_to_all.21 = bf16[16,16,1024]{2,1,0:T(8,128)(2,1)S(1)} all-to-all(bf16[16,16,1024]{2,1,0:T(8,128)(2,1)S(1)} %bitcast.25), channel_id=1, replica_groups=mesh['plane'=8,'spot'=16,'tp'=2] {'spot'}, dimensions={0} | all-to-all | bytes 1048576 | tf_op jit(solution)/shard_map/all_to_all | solution.py:399
  46.2 0.0 collective-permute-done.1.gate_hbm
  46.2 0.0 collective-permute-done.2.up_hbm
  46.2 0.0 collective-permute-done.3.down_hbm
  46.2 3.4 %expert.1 = bf16[256,1024]{1,0:T(8,128)(2,1)S(1)} custom-call(bf16[256,1024]{1,0:T(8,128)(2,1)S(1)} %bitcast.16, bf16[448,1024]{1,0:T(8,128)(2,1)S(1)} %bitcast.19, bf16[448,1024]{1,0:T(8,128)(2,1)S(1)} %bitcast.21, bf16[448,1024]{1,0:T(8,128)(2,1)S(1)} %copy-done.2, bf16[448,1024]{1,0:T(8,128)(2,1)} %collective-permute-done.1.gate_hbm, ...), custom_call_target="tpu_custom_call" | custom-call | tf_op jit(solution)/shard_map/expert/pallas_call | solution.py:342
  49.6 11.6 %all_to_all.22 = bf16[16,16,1024]{2,1,0:T(8,128)(2,1)S(1)} all-to-all(bf16[16,16,1024]{2,1,0:T(8,128)(2,1)S(1)} %bitcast.17), channel_id=1, replica_groups=mesh['plane'=8,'spot'=16,'tp'=2] {'spot'}, dimensions={0} | all-to-all | bytes 1048576 | tf_op jit(solution)/shard_map/all_to_all | solution.py:399
  61.2 0.1 bitcast_reduce_fusion
  61.3 0.1 copy.30
  61.4 14.6 %all_to_all.23 = bf16[16,4,512]{2,1,0:T(4,128)(2,1)S(1)} all-to-all(bf16[16,4,512]{2,1,0:T(4,128)(2,1)S(1)} %reshape.52), channel_id=1, replica_groups=mesh['plane'=8,'spot'=16,'tp'=2] {'plane','tp'}, dimensions={0} | all-to-all | bytes 131072 | tf_op jit(solution)/shard_map/all_to_all | solution.py:399
  76.0 0.7 mix.1
  (8 shorter events, 0.2 us)
Async XLA Ops:
  0.6 6.9 %copy-start = (bf16[1024,448]{0,1:T(8,128)(2,1)S(1)}, bf16[1024,448]{0,1:T(8,128)(2,1)}, u32[]{:S(2)}) copy-start(bf16[1024,448]{0,1:T(8,128)(2,1)} %param.29) | copy-start | bytes 2752516
  0.6 10.2 %copy-start.1 = (bf16[1024,448]{0,1:T(8,128)(2,1)S(1)}, bf16[1024,448]{0,1:T(8,128)(2,1)}, u32[]{:S(2)}) copy-start(bf16[1024,448]{0,1:T(8,128)(2,1)} %param.30) | copy-start | bytes 2752516
  0.7 10.3 %copy-start.2 = (bf16[448,1024]{1,0:T(8,128)(2,1)S(1)}, bf16[448,1024]{1,0:T(8,128)(2,1)}, u32[]{:S(2)}) copy-start(bf16[448,1024]{1,0:T(8,128)(2,1)} %down_own.1) | copy-start | bytes 2752516
  0.7 15.1 %copy-start.3 = (bf16[16,1024]{1,0:T(8,128)(2,1)S(1)}, bf16[16,1024]{1,0:T(8,128)(2,1)}, u32[]{:S(2)}) copy-start(bf16[16,1024]{1,0:T(8,128)(2,1)} %tokens.1) | copy-start | bytes 98308
  0.7 15.0 %copy-start.4 = (s32[2048,2]{0,1:T(2,128)S(1)}, s32[2048,2]{0,1:T(2,128)}, u32[]{:S(2)}) copy-start(s32[2048,2]{0,1:T(2,128)} %param.18) | copy-start | bytes 49156
  0.7 15.0 %copy-start.5 = (f32[2048,2]{0,1:T(2,128)S(1)}, f32[2048,2]{0,1:T(2,128)}, u32[]{:S(2)}) copy-start(f32[2048,2]{0,1:T(2,128)} %param.19) | copy-start | bytes 49156
  0.7 15.0 %copy-start.6 = (f32[1024]{0:T(1024)S(1)}, f32[1024]{0:T(1024)}, u32[]{:S(2)}) copy-start(f32[1024]{0:T(1024)} %param.28) | copy-start | bytes 12292
  7.6 38.6 %collective-permute-start.1 = (bf16[448,1024]{1,0:T(8,128)(2,1)S(1)}, bf16[448,1024]{1,0:T(8,128)(2,1)}, u32[]{:S(2)}, u32[]{:S(2)}) collective-permute-start(bf16[448,1024]{1,0:T(8,128)(2,1)S(1)} %bitcast.18), channel_id=1, source_target_pairs={{0,1},{1,0},{2,3},{3,2},{4,5},{5,4},{6,7},{7,6},{8,9},{9,8},{10,11... | collective-permute-start | bytes 2752520 | tf_op jit(solution)/shard_map/ppermute | solution.py:396
  10.9 35.3 %collective-permute-start.2 = (bf16[448,1024]{1,0:T(8,128)(2,1)S(1)}, bf16[448,1024]{1,0:T(8,128)(2,1)}, u32[]{:S(2)}, u32[]{:S(2)}) collective-permute-start(bf16[448,1024]{1,0:T(8,128)(2,1)S(1)} %bitcast.20), channel_id=1, source_target_pairs={{0,1},{1,0},{2,3},{3,2},{4,5},{5,4},{6,7},{7,6},{8,9},{9,8},{10,11... | collective-permute-start | bytes 2752520 | tf_op jit(solution)/shard_map/ppermute | solution.py:396
  11.0 35.2 %collective-permute-start.3 = (bf16[448,1024]{1,0:T(8,128)(2,1)S(1)}, bf16[448,1024]{1,0:T(8,128)(2,1)}, u32[]{:S(2)}, u32[]{:S(2)}) collective-permute-start(bf16[448,1024]{1,0:T(8,128)(2,1)S(1)} %copy-done.2), channel_id=1, source_target_pairs={{0,1},{1,0},{2,3},{3,2},{4,5},{5,4},{6,7},{7,6},{8,9},{9,8},{10,11... | collective-permute-start | bytes 2752520 | tf_op jit(solution)/shard_map/ppermute | solution.py:396
  11.4 4.3 %collective-permute-start = (bf16[16,1024]{1,0:T(8,128)(2,1)S(1)}, bf16[16,1024]{1,0:T(8,128)(2,1)S(1)}, u32[]{:S(2)}, u32[]{:S(2)}) collective-permute-start(bf16[16,1024]{1,0:T(8,128)(2,1)S(1)} %get-tuple-element.12.own), channel_id=1, source_target_pairs={{0,1},{1,0},{2,3},{3,2},{4,5},{5,4},{6,7},{7,6},{8,9},{9,8},{10,11... | collective-permute-start | bytes 98312 | tf_op jit(solution)/shard_map/ppermute | solution.py:396
